TPU v7x, 512 devices: a whole 4x8x8 slice. The times are simulated.
512 devices in a mesh: gr: 2 (over z_hi), sp: 32 (over z_lo, y), tp: 8 (over x, core).
Axes of the slice: x: 4, y: 8, z: 8 (z_hi: 2, z_lo: 4; z = z_hi * 4 + z_lo), core: 2. Of those that a mesh axis runs over, the one named last changes fastest.
Arguments:
- mixer_input: bfloat16 [64, 6144, 2048], P(('gr', 'tp'), 'sp'), may hold values from -16.8 to 16.8
- key_weight: bfloat16 [2048, 256], P('tp'), may hold values from -0.125 to 0.125
- content_projection_matrix: bfloat16 [2048, 256], P('tp'), may hold values from -0.125 to 0.125
- new_queries: bfloat16 [64, 32, 64], P(('gr', 'sp'), 'tp'), may hold values from -6 to 6
- head_stick_offset: float32 [32], replicated, may hold values from -11 to -4
Outputs:
- kv_cache: bfloat16 [64, 8, 6144, 128], P(('gr', 'sp'), 'tp')
- initial_attended_output: bfloat16 [64, 32, 64], P(('gr', 'sp'), 'tp')
All inputs are finite; a program needn't handle non-finite values.
Results may differ from a plain program's by a relative error of at most 0.0081.
Values may be sent and summed in bfloat16 or wider, within the bound.
No kernel may reach another device: no remote copies, remote signals or barrier semaphores. Data moves between devices by JAX's collectives and lax.ppermute only.
A program may use at most 64 MiB of HBM per device.

v0:
```python
import jax
import jax.numpy as jnp
from jax import lax
from jax.sharding import PartitionSpec as P

HEAD_DIM = 64


def laid_out(blocks, dim):
    blocks = jnp.moveaxis(blocks, 0, dim)
    lengths = blocks.shape
    return blocks.reshape(*lengths[:dim], lengths[dim] * lengths[dim + 1], *lengths[dim + 2 :])


def copy_for_each(shard, axis):
    copies = jnp.broadcast_to(shard, (lax.axis_size(axis), *shard.shape))
    return lax.all_to_all(copies, axis, split_axis=0, concat_axis=0, tiled=True)


def collect(shard, axis, dim):
    return laid_out(copy_for_each(shard, axis), dim)


def side_by_side(arrays, axis, dim, along):
    ends, at = ([], 0)
    for a in arrays[:-1]:
        at += a.shape[along]
        ends.append(at)
    both = jnp.concatenate(arrays, axis=along)
    return tuple(jnp.split(collect(both, axis, dim), ends, axis=along))


def local(mixer_input, key_weight, content_projection_matrix, new_queries, head_stick_offset):
    group_seqs, block_rows, model_width = mixer_input.shape
    key_heads = key_weight.shape[1] // HEAD_DIM
    head_devices = lax.axis_size("tp")
    copies = max(1, head_devices // key_heads)
    input_rows = mixer_input.reshape(group_seqs * block_rows, model_width)
    pieces = side_by_side((key_weight, content_projection_matrix), "tp", 0, 1)
    key_sum = jnp.dot(input_rows, pieces[0], preferred_element_type=jnp.float32)
    value_sum = jnp.dot(input_rows, pieces[1], preferred_element_type=jnp.float32)
    key_rows = key_sum.astype(jnp.bfloat16).reshape(group_seqs, block_rows, key_heads, HEAD_DIM)
    value_rows = value_sum.astype(jnp.bfloat16).reshape(group_seqs, block_rows, key_heads, HEAD_DIM)
    stacked = jnp.concatenate([key_rows, value_rows], axis=3).transpose(0, 2, 1, 3)
    spread = jnp.repeat(stacked, copies, axis=1)
    spread = lax.all_to_all(spread, "tp", split_axis=1, concat_axis=0, tiled=True)
    kv_cache = lax.all_to_all(spread, "sp", split_axis=0, concat_axis=2, tiled=True)
    seq_local = kv_cache.shape[0]
    slot_local = kv_cache.shape[1]
    head_local = new_queries.shape[1]
    inverse_root = HEAD_DIM ** (-0.5)
    offset_values = lax.dynamic_slice_in_dim(
        head_stick_offset, lax.axis_index("tp") * head_local, head_local
    )
    grouped = new_queries.reshape(seq_local, slot_local, head_local // slot_local, HEAD_DIM)
    cache_keys = kv_cache[:, :, :, :HEAD_DIM]
    cache_values = kv_cache[:, :, :, HEAD_DIM:]
    logit_scores = (
        jnp.einsum("bhgd,bhsd->bhgs", grouped, cache_keys, preferred_element_type=jnp.float32)
        * inverse_root
    )
    logit_scores = logit_scores + offset_values.reshape(1, slot_local, -1, 1)
    stay_terms = jax.nn.log_sigmoid(-logit_scores)
    later_terms = lax.cumsum(stay_terms, axis=3, reverse=True) - stay_terms
    weights = jnp.exp(jax.nn.log_sigmoid(logit_scores) + later_terms).astype(jnp.bfloat16)
    result = jnp.einsum(
        "bhgs,bhsd->bhgd", weights, cache_values, preferred_element_type=jnp.float32
    )
    initial_attended_output = result.reshape(seq_local, head_local, HEAD_DIM).astype(jnp.bfloat16)
    return (kv_cache, initial_attended_output)


def solution(mesh):
    return jax.shard_map(
        local,
        mesh=mesh,
        in_specs=(
            P(("gr", "tp"), "sp", None),
            P("tp", None),
            P("tp", None),
            P(("gr", "sp"), "tp", None),
            P(),
        ),
        out_specs=(P(("gr", "sp"), "tp", None, None), P(("gr", "sp"), "tp", None)),
        check_vma=False,
    )
```

profile of v0, /device:TPU:8, one launch (start us, length us, event | category | flops | bytes accessed | tf_op | source)
XLA Modules:
  0.0 139.9 jit_solution(13223402609899126694)
XLA Ops:
  0.6 0.0 copy-start
  0.6 1.1 pad_maximum_fusion
  1.8 0.2 broadcast_in_dim.6
  2.0 31.3 %all_to_all.35 = bf16[8,256,512]{2,1,0:T(8,128)(2,1)S(1)} all-to-all(bf16[8,256,512]{2,1,0:T(8,128)(2,1)S(1)} %broadcast_in_dim.6), channel_id=1, replica_groups=mesh['gr'=2,'sp'=32,'tp'=8] {'tp'}, dimensions={0} | all-to-all | bytes 4194304 | tf_op jit(solution)/shard_map/all_to_all | solution.py:17
  33.3 0.0 copy-done
  33.3 1.8 %fusion.3 = bf16[768,256]{0,1:T(8,128)(2,1)} fusion(bf16[768,2048]{1,0:T(8,128)(2,1)S(1)} %bitcast.61, bf16[2048,512]{1,0:T(8,128)(2,1)S(1)} %bitcast.65), kind=kOutput, calls=%fused_computation.8 | convolution fusion | flops 805502976 | bytes 4587520 | tf_op jit(solution)/shard_map/dot_general | solution.py:40
  35.1 1.1 fusion.4
  36.2 2.3 %reshape.91 = bf16[4,192,4,64]{1,0,3,2:T(4,128)(2,1)} reshape(bf16[768,256]{0,1:T(8,128)(2,1)} %fusion.3) | data formatting | bytes 786432 | tf_op jit(solution)/shard_map/reshape | solution.py:42
  38.5 1.3 reshape.92
  39.8 2.9 %maximum_bitcast_fusion = bf16[4,4,192,128]{2,0,3,1:T(4,128)(2,1)} fusion(bf16[4,192,4,64]{1,0,3,2:T(4,128)(2,1)} %reshape.92, bf16[4,192,4,64]{1,0,3,2:T(4,128)(2,1)} %reshape.91), kind=kLoop, calls=%fused_computation.14 | loop fusion | flops 393216 | bytes 1572864 | tf_op jit(solution)/shard_map/transpose | solution.py:44
  42.7 2.3 %copy.9 = bf16[4,4,192,128]{3,2,0,1:T(8,128)(2,1)} copy(bf16[4,4,192,128]{2,0,3,1:T(4,128)(2,1)} %maximum_bitcast_fusion) | data formatting | bytes 1572864 | tf_op jit(solution)/shard_map/transpose | solution.py:44
  45.0 1.5 %broadcast_in_dim.7 = bf16[4,4,2,192,128]{4,3,0,2,1:T(8,128)(2,1)S(1)} broadcast(bf16[4,4,192,128]{3,2,0,1:T(8,128)(2,1)} %copy.9), dimensions={0,1,3,4} | broadcast | bytes 2359296 | tf_op jit(solution)/shard_map/broadcast_in_dim | solution.py:45
  46.5 24.7 %all_to_all.36 = bf16[4,8,192,128]{3,2,0,1:T(8,128)(2,1)} all-to-all(bf16[4,8,192,128]{3,2,0,1:T(8,128)(2,1)S(1)} %bitcast.64), channel_id=1, replica_groups=mesh['gr'=2,'sp'=32,'tp'=8] {'tp'}, dimensions={1} | all-to-all | bytes 3145728 | tf_op jit(solution)/shard_map/all_to_all | solution.py:46
  71.2 0.0 copy-start.2
  71.2 0.0 copy-start.1
  71.2 13.3 %all-to-all-start.2 = ((bf16[32,1,192,128]{3,2,1,0:T(8,128)(2,1)}), bf16[32,1,192,128]{3,2,1,0:T(8,128)(2,1)}, u32[]{:S(2)}, u32[]{:S(2)}) async-start(bf16[32,1,192,128]{3,2,1,0:T(8,128)(2,1)} %bitcast.63), calls=%async_computation.2 | async-start | bytes 3145728 | tf_op jit(solution)/shard_map/all_to_all | solution.py:47
  84.6 0.0 copy-done.2
  84.6 0.1 dynamic_slice.3
  84.7 42.1 %all-to-all-done.2 = bf16[32,1,192,128]{3,2,1,0:T(8,128)(2,1)} async-done(((bf16[32,1,192,128]{3,2,1,0:T(8,128)(2,1)}), bf16[32,1,192,128]{3,2,1,0:T(8,128)(2,1)}, u32[]{:S(2)}, u32[]{:S(2)}) %all-to-all-start.2) | async-done | bytes 1572896 | tf_op jit(solution)/shard_map/all_to_all | solution.py:47
  126.7 0.0 copy-done.1
  126.7 1.9 %fusion.1 = f32[4,6144]{1,0:T(4,128)S(1)} fusion(bf16[1,1,6144,128]{3,2,1,0:T(8,128)(2,1)} %bitcast.9, f32[4]{0:T(128)S(1)} %dynamic_slice.3, bf16[1,4,64]{2,1,0:T(4,128)(2,1)S(1)} %copy-done.1), kind=kOutput, calls=%fused_computation.2 | convolution fusion | flops 3194880 | bytes 1671696 | tf_op jit(solution)/shard_map/bhgd,bhsd->bhgs/dot_general | solution.py:59
  128.6 0.1 fusion.18
  128.8 5.0 %reduce-window.6 = f32[1,1,4,48,128]{4,3,2,1,0:T(8,128)S(1)} reduce-window(f32[1,1,4,48,128]{4,3,2,1,0:T(8,128)S(1)} %bitcast.68, f32[]{:T(128)} %constant.18.clone.1), window={size=1x1x1x1x128 pad=0_0x0_0x0_0x0_0x0_127}, to_apply=%region_0.1 | reduce-window | flops 3121152 | bytes 196612 | tf_op jit(solution)/shard_map/reduce-window
  133.8 0.1 slice_reduce_fusion
  133.9 0.3 reduce-window.9
  134.2 0.1 slice_bitcast_fusion.8
  134.3 0.1 broadcast_bitcast_fusion
  134.4 2.8 %fusion.6 = bf16[1,4,64]{2,1,0:T(4,128)(2,1)} fusion(bf16[1,1,6144,128]{3,2,1,0:T(8,128)(2,1)} %bitcast.9, f32[1,4,48,128]{3,2,1,0:T(8,128)S(1)} %broadcast_bitcast_fusion, f32[1,4,48,128]{3,2,1,0:T(8,128)S(1)} %bitcast.67, f32[4,6144]{1,0:T(4,128)S(1)} %fusion.1), kind=kOutput, calls=%fused_computation.11 | convolution fusion | flops 3612928 | bytes 1868288 | tf_op jit(solution)/shard_map/bhgs,bhsd->bhgd/dot_general | solution.py:66
  137.2 2.7 %copy.20 = bf16[1,1,6144,128]{3,2,1,0:T(8,128)(2,1)} copy(bf16[1,1,6144,128]{3,2,1,0:T(8,128)(2,1)} %bitcast.9) | data formatting | bytes 3145728
  (1 shorter events, 0.0 us)
Async XLA Ops:
  0.6 32.6 %copy-start = (bf16[4,192,2048]{2,1,0:T(8,128)(2,1)S(1)}, bf16[4,192,2048]{2,1,0:T(8,128)(2,1)}, u32[]{:S(2)}) copy-start(bf16[4,192,2048]{2,1,0:T(8,128)(2,1)} %param.5) | copy-start | bytes 9437188
  71.2 13.3 %copy-start.2 = (f32[32]{0:T(128)S(1)}, f32[32]{0:T(128)}, u32[]{:S(2)}) copy-start(f32[32]{0:T(128)} %param.9) | copy-start | bytes 388
  71.2 55.5 %copy-start.1 = (bf16[1,4,64]{2,1,0:T(4,128)(2,1)S(1)}, bf16[1,4,64]{2,1,0:T(4,128)(2,1)}, u32[]{:S(2)}) copy-start(bf16[1,4,64]{2,1,0:T(4,128)(2,1)} %param.8) | copy-start | bytes 1540
  71.2 55.5 %all-to-all-start.2 = ((bf16[32,1,192,128]{3,2,1,0:T(8,128)(2,1)}), bf16[32,1,192,128]{3,2,1,0:T(8,128)(2,1)}, u32[]{:S(2)}, u32[]{:S(2)}) async-start(bf16[32,1,192,128]{3,2,1,0:T(8,128)(2,1)} %bitcast.63), calls=%async_computation.2 | async-start | bytes 3145728 | tf_op jit(solution)/shard_map/all_to_all | solution.py:47
where the time goes:
time: 140 us
  blocking collectives  56 us (40%)
  waiting for transfers between devices  42.1 us (30%)
  starting transfers between devices  13.3 us (10%)
  local copies, waits for them, and re-layouts  10.6 us (8%)
  other arithmetic  9.54 us (7%)
  matrix products  7.62 us (5%)
    all_to_all x1, waiting for transfers between devices, local(): lax.all_to_all(spread, 'sp', split_axis=0, concat_axis=2, tiled=True)  42.1 us
    all_to_all x1, blocking collectives, copy_for_each(): return lax.all_to_all(copies, axis, split_axis=0, concat_axis=0, tiled=True)  31.3 us
    all_to_all x1, blocking collectives, local(): lax.all_to_all(spread, 'tp', split_axis=1, concat_axis=0, tiled=True)  24.7 us
    all_to_all x1, starting transfers between devices, local(): lax.all_to_all(spread, 'sp', split_axis=0, concat_axis=2, tiled=True)  13.3 us
    another operation x2, other arithmetic  5.35 us
    transpose x1, other arithmetic, local(): jnp.concatenate([key_rows, value_rows], axis=3).transpose(0, 2, 1, 3)  2.91 us
  transfers between devices with their start and end apart: 1, of which 1 were waited for; matrix products, arithmetic and copies ran while one was open for 0% of the time, Pallas kernels for 0%

commit v1 on v0

v1 whole, which is shorter than its diff:
```python
import functools

import jax
import jax.numpy as jnp
from jax import lax
from jax.experimental import pallas as pl
from jax.experimental.pallas import tpu as pltpu
from jax.sharding import Mesh, PartitionSpec as P

HEAD_DIM = 64
F32, BF16 = jnp.float32, jnp.bfloat16


def project_kernel(core_ref, x_ref, mine_ref, other_ref, out_ref):
    shards, depth, width = mine_ref.shape
    seqs, half = out_ref.shape[1], out_ref.shape[2]
    core = core_ref[0]
    total = None
    for s in range(shards):
        for ref, which in ((mine_ref, core), (other_ref, 1 - core)):
            at = pl.multiple_of((2 * s + which) * depth, depth)
            part = jnp.dot(x_ref[:, pl.ds(at, depth)], ref[s], preferred_element_type=F32)
            total = part if total is None else total + part
    rows = total.astype(BF16)
    for slot in range(out_ref.shape[0]):
        for i in range(seqs):
            start = (2 * i + slot % 2) * half
            head = slot // 2
            out_ref[slot, i] = rows[start : start + half, 128 * head : 128 * head + 128]


def project(core, x, mine, other, seqs, half):
    heads = mine.shape[2] // 128
    return pl.pallas_call(
        project_kernel,
        out_shape=jax.ShapeDtypeStruct((2 * heads, seqs, half, 128), BF16),
        in_specs=[pl.BlockSpec(memory_space=pltpu.SMEM)] + [pl.BlockSpec(memory_space=pltpu.VMEM)] * 3,
        out_specs=pl.BlockSpec(memory_space=pltpu.VMEM),
        cost_estimate=pl.CostEstimate(flops=2 * x.shape[0] * x.shape[1] * mine.shape[2], bytes_accessed=8 << 20, transcendentals=0),
    )(core, x, mine, other)


def split3(a):
    hi = a.astype(BF16)
    rest = a - hi.astype(F32)
    mid = rest.astype(BF16)
    return hi, mid, (rest - mid.astype(F32)).astype(BF16)


def read_kernel(core_ref, mine_ref, other_ref, q_ref, off_ref, kv_ref, out_ref):
    blocks, half, width = mine_ref.shape
    span = kv_ref.shape[2]
    rows = q_ref.shape[0]
    core = core_ref[0]
    for b in range(blocks):
        base = 2 * half * b
        kv_ref[0, 0, pl.ds(pl.multiple_of(base + core * half, half), half)] = mine_ref[b]
        kv_ref[0, 0, pl.ds(pl.multiple_of(base + (1 - core) * half, half), half)] = other_ref[b]
    tiles = span // 128
    scores = lax.dot_general(q_ref[...], kv_ref[0, 0], (((1,), (1,)), ((), ())), preferred_element_type=F32)
    z = scores * (HEAD_DIM ** -0.5) + off_ref[:, :1]
    stay = -(jnp.maximum(z, 0.0) + jnp.log1p(jnp.exp(-jnp.abs(z))))
    stacked = jnp.concatenate([stay[:, 128 * t : 128 * t + 128] for t in range(tiles)], axis=0)
    r = lax.broadcasted_iota(jnp.int32, (128, 128), 0)
    c = lax.broadcasted_iota(jnp.int32, (128, 128), 1)
    from_here = (r >= c).astype(F32).astype(BF16)
    suffix = None
    for piece in split3(stacked):
        part = jnp.dot(piece, from_here, preferred_element_type=F32)
        suffix = part if suffix is None else suffix + part
    later = jnp.zeros((rows, 1), F32)
    pieces = [None] * tiles
    for t in reversed(range(tiles)):
        own = suffix[rows * t : rows * t + rows]
        pieces[t] = own + later
        later = later + own[:, :1]
    log_weight = z + jnp.concatenate(pieces, axis=1)
    weight = jnp.exp(log_weight).astype(BF16)
    out_ref[...] = jnp.dot(weight, kv_ref[0, 0], preferred_element_type=F32)


def read(core, mine, other, q, off):
    blocks, half, width = mine.shape
    span = 2 * blocks * half
    rows = q.shape[0]
    return pl.pallas_call(
        read_kernel,
        out_shape=(jax.ShapeDtypeStruct((1, 1, span, width), BF16), jax.ShapeDtypeStruct((rows, width), F32)),
        in_specs=[pl.BlockSpec(memory_space=pltpu.SMEM)] + [pl.BlockSpec(memory_space=pltpu.VMEM)] * 4,
        out_specs=(pl.BlockSpec(memory_space=pltpu.VMEM), pl.BlockSpec(memory_space=pltpu.VMEM)),
        cost_estimate=pl.CostEstimate(flops=4 * rows * span * width, bytes_accessed=4 << 20, transcendentals=3 * rows * span),
    )(core, mine, other, q, off)


def local(mixer_input, key_weight, content_projection_matrix, new_queries, head_stick_offset):
    seqs, block, width = mixer_input.shape
    depth, columns = key_weight.shape
    heads = columns // HEAD_DIM
    half = block // 2
    core = lax.axis_index("core")
    core_arg = core.reshape(1).astype(jnp.int32)
    other = [(0, 1), (1, 0)]
    weight = jnp.concatenate(
        [key_weight.reshape(depth, heads, HEAD_DIM), content_projection_matrix.reshape(depth, heads, HEAD_DIM)], axis=2
    ).reshape(depth, 2 * columns)
    chips = lax.axis_size("x")
    mine = lax.all_to_all(jnp.broadcast_to(weight, (chips, *weight.shape)), "x", 0, 0, tiled=True)
    theirs = lax.ppermute(mine, "core", other)
    rows = project(core_arg, mixer_input.reshape(seqs * block, width), mine, theirs, seqs, half)
    rows = lax.all_to_all(rows, ("x", "core"), 0, 0, tiled=True)
    rows = rows.reshape(rows.shape[0] * seqs, half, 128)
    mine = lax.all_to_all(rows, ("z", "y"), 0, 0, tiled=True)
    theirs = lax.ppermute(mine, "core", other)
    group = new_queries.shape[1]
    start = (lax.axis_index("x") * 2 + core) * group
    offset = lax.dynamic_slice_in_dim(head_stick_offset, start, group)
    q = jnp.pad(new_queries[0], ((0, 8 - group), (0, 128 - HEAD_DIM)))
    off = jnp.broadcast_to(jnp.pad(offset, (0, 8 - group))[:, None], (8, 128))
    kv_cache, read_out = read(core_arg, mine, theirs, q, off)
    return kv_cache, read_out[None, :group, HEAD_DIM:].astype(BF16)


def solution(mesh):
    sizes = dict(mesh.shape)
    wide = Mesh(mesh.devices.reshape(sizes["gr"], 4, 8, 4, 2), ("gr", "z", "y", "x", "core"))
    sp, tp = ("z", "y"), ("x", "core")
    return jax.shard_map(
        local,
        mesh=wide,
        in_specs=(
            P(("gr", *tp), sp, None),
            P(tp, None),
            P(tp, None),
            P(("gr", *sp), tp, None),
            P(),
        ),
        out_specs=(P(("gr", *sp), tp, None, None), P(("gr", *sp), tp, None)),
        check_vma=False,
    )
```

time: 140 us -> 97 us (0.69)
  the two profiles are of different devices: /device:TPU:8 before, /device:TPU:1 now
where the time goes in v1:
time: 97 us; the launch traced here: 96.6 us
  blocking collectives  64.1 us (66%)
  starting transfers between devices  13.7 us (14%)
  Pallas kernels  8.56 us (9%)
  local copies, waits for them, and re-layouts  5.4 us (6%)
  waiting for transfers between devices  3.46 us (4%)
    all_to_all x1, blocking collectives, local(): mine = lax.all_to_all(rows, ('z', 'y'), 0, 0, tiled=True)  32.9 us
    all_to_all x1, blocking collectives, local(): rows = lax.all_to_all(rows, ('x', 'core'), 0, 0, tiled=True)  16 us
    all_to_all x1, blocking collectives, local(): lax.all_to_all(jnp.broadcast_to(weight, (chips, *weight.shape)), 'x', 0,...  15.2 us
    ppermute x2, starting transfers between devices, local(): theirs = lax.ppermute(mine, 'core', other)  13.7 us
    pallas_call x1, Pallas kernels, project(): pl.pallas_call(project_kernel, out_shape=jax.ShapeDtypeStruct((2 * heads,...  5.22 us
    ppermute x2, waiting for transfers between devices, local(): theirs = lax.ppermute(mine, 'core', other)  3.46 us
    pallas_call x1, Pallas kernels, read(): pl.pallas_call(read_kernel, out_shape=(jax.ShapeDtypeStruct((1, 1, span,...  3.34 us
    unnamed x14, local copies, waits for them, and re-layouts  3.16 us
  transfers between devices with their start and end apart: 2, of which 2 were waited for; matrix products, arithmetic and copies ran while one was open for 1% of the time, Pallas kernels for 0%

profile of v1, /device:TPU:1, one launch (start us, length us, event | category | flops | bytes accessed | tf_op | source)
XLA Modules:
  0.0 96.6 jit_solution(5960842381479355120)
XLA Ops:
  0.6 1.0 %copy.7 = bf16[256,256]{0,1:T(8,128)(2,1)S(1)} copy(bf16[256,256]{1,0:T(8,128)(2,1)} %param.6) | data formatting | bytes 262144 | tf_op args[1]
  1.6 1.0 %copy.8 = bf16[256,256]{0,1:T(8,128)(2,1)S(1)} copy(bf16[256,256]{1,0:T(8,128)(2,1)} %param.7) | data formatting | bytes 262144 | tf_op args[2]
  2.7 0.1 copy.9
  2.8 0.1 broadcast_in_dim.4
  2.9 15.2 %all_to_all.15.mine_ref = bf16[4,256,512]{2,1,0:T(8,128)(2,1)S(1)} all-to-all(bf16[4,256,512]{2,1,0:T(8,128)(2,1)S(1)} %broadcast_in_dim.4), channel_id=1, replica_groups=mesh['gr'=2,'z'=4,'y'=8,'x'=4,'core'=2] {'x'}, dimensions={0} | all-to-all | bytes 2097152 | tf_op jit(solution)/shard_map/all_to_all | solution.py:107
  18.1 0.0 copy-start
  18.1 7.4 %collective-permute-start = (bf16[4,256,512]{2,1,0:T(8,128)(2,1)S(1)}, bf16[4,256,512]{2,1,0:T(8,128)(2,1)S(1)}, u32[]{:S(2)}, u32[]{:S(2)}) collective-permute-start(bf16[4,256,512]{2,1,0:T(8,128)(2,1)S(1)} %all_to_all.15.mine_ref), channel_id=1, source_target_pairs={{0,1},{1,0},{2,3},{3,2},{4,5},{5,4},{6,7},{7,6},{8,9},{9,8},{10,11... | collective-permute-start | bytes 3145736 | tf_op jit(solution)/shard_map/ppermute | solution.py:108
  25.5 2.3 %collective-permute-done.other_ref = bf16[4,256,512]{2,1,0:T(8,128)(2,1)S(1)} collective-permute-done((bf16[4,256,512]{2,1,0:T(8,128)(2,1)S(1)}, bf16[4,256,512]{2,1,0:T(8,128)(2,1)S(1)}, u32[]{:S(2)}, u32[]{:S(2)}) %collective-permute-start) | collective-permute-done | bytes 1048608 | tf_op jit(solution)/shard_map/ppermute | solution.py:108
  27.8 0.0 copy-start.2
  27.8 0.0 copy-done
  27.8 1.0 copy-done.2
  28.7 0.0 copy-start.5
  28.7 0.0 copy-start.4
  28.7 5.2 %shard_map.68 = bf16[8,4,96,128]{3,2,1,0:T(8,128)(2,1)} custom-call(s32[1]{0:T(128)} %bitcast.core_ref, bf16[768,2048]{1,0:T(8,128)(2,1)} %bitcast.9, bf16[4,256,512]{2,1,0:T(8,128)(2,1)} %copy-done, bf16[4,256,512]{2,1,0:T(8,128)(2,1)} %copy-done.2), custom_call_target="tpu_custom_call" | custom-call | flops 1610612736 | bytes 8388608 | tf_op jit(solution)/shard_map/pallas_call | solution.py:34
  34.0 16.0 %all_to_all.16 = bf16[8,4,96,128]{3,2,1,0:T(8,128)(2,1)S(1)} all-to-all(bf16[8,4,96,128]{3,2,1,0:T(8,128)(2,1)} %shard_map.68), channel_id=1, replica_groups=mesh['gr'=2,'z'=4,'y'=8,'x'=4,'core'=2] {'x','core'}, dimensions={0} | all-to-all | bytes 1572864 | tf_op jit(solution)/shard_map/all_to_all | solution.py:110
  49.9 32.9 %all_to_all.17.mine_ref = bf16[32,96,128]{2,1,0:T(8,128)(2,1)S(1)} all-to-all(bf16[32,96,128]{2,1,0:T(8,128)(2,1)S(1)} %bitcast.10), channel_id=1, replica_groups=mesh['gr'=2,'z'=4,'y'=8,'x'=4,'core'=2] {'z','y'}, dimensions={0} | all-to-all | bytes 1572864 | tf_op jit(solution)/shard_map/all_to_all | solution.py:112
  82.8 0.0 copy-start.1
  82.8 6.3 %collective-permute-start.1 = (bf16[32,96,128]{2,1,0:T(8,128)(2,1)S(1)}, bf16[32,96,128]{2,1,0:T(8,128)(2,1)S(1)}, u32[]{:S(2)}, u32[]{:S(2)}) collective-permute-start(bf16[32,96,128]{2,1,0:T(8,128)(2,1)S(1)} %all_to_all.17.mine_ref), channel_id=1, source_target_pairs={{0,1},{1,0},{2,3},{3,2},{4,5},{5,4},{6,7},{7,6},{8,9},{9,8},{10,11... | collective-permute-start | bytes 2359304 | tf_op jit(solution)/shard_map/ppermute | solution.py:113
  89.2 0.0 copy-done.5
  89.2 0.1 dynamic_slice.3
  89.2 0.0 copy-done.4
  89.2 0.6 pad.8.q_ref
  89.8 1.2 %collective-permute-done.1.other_ref = bf16[32,96,128]{2,1,0:T(8,128)(2,1)S(1)} collective-permute-done((bf16[32,96,128]{2,1,0:T(8,128)(2,1)S(1)}, bf16[32,96,128]{2,1,0:T(8,128)(2,1)S(1)}, u32[]{:S(2)}, u32[]{:S(2)}) %collective-permute-start.1) | collective-permute-done | bytes 786464 | tf_op jit(solution)/shard_map/ppermute | solution.py:113
  91.0 0.0 copy-start.3
  91.0 0.7 broadcast_in_dim.5.off_ref
  91.8 0.0 copy-done.1
  91.8 0.2 copy-done.3
  91.9 3.3 %shard_map.69 = (bf16[1,1,6144,128]{3,2,1,0:T(8,128)(2,1)}, f32[8,128]{1,0:T(8,128)}) custom-call(s32[1]{0:T(128)} %bitcast.core_ref, bf16[32,96,128]{2,1,0:T(8,128)(2,1)} %copy-done.1, bf16[32,96,128]{2,1,0:T(8,128)(2,1)} %copy-done.3, bf16[8,128]{1,0:T(8,128)(2,1)} %pad.8.q_ref, f32[8,128]{1,0:T(8,128)} %broadcast_in_dim.5.off_ref), custom_call_target="tpu_custom_call" | custom-call | flops 25165824 | bytes 4194304 | tf_op jit(solution)/shard_map/pallas_call | solution.py:86
  95.3 0.7 convert.3
  96.0 0.6 slice_bitcast_fusion
  (2 shorter events, 0.0 us)
Async XLA Ops:
  18.1 9.7 %copy-start = (bf16[4,256,512]{2,1,0:T(8,128)(2,1)}, bf16[4,256,512]{2,1,0:T(8,128)(2,1)S(1)}, u32[]{:S(2)}) copy-start(bf16[4,256,512]{2,1,0:T(8,128)(2,1)S(1)} %all_to_all.15.mine_ref) | copy-start | bytes 3145732
  18.1 9.7 %collective-permute-start = (bf16[4,256,512]{2,1,0:T(8,128)(2,1)S(1)}, bf16[4,256,512]{2,1,0:T(8,128)(2,1)S(1)}, u32[]{:S(2)}, u32[]{:S(2)}) collective-permute-start(bf16[4,256,512]{2,1,0:T(8,128)(2,1)S(1)} %all_to_all.15.mine_ref), channel_id=1, source_target_pairs={{0,1},{1,0},{2,3},{3,2},{4,5},{5,4},{6,7},{7,6},{8,9},{9,8},{10,11... | collective-permute-start | bytes 3145736 | tf_op jit(solution)/shard_map/ppermute | solution.py:108
  27.8 1.0 %copy-start.2 = (bf16[4,256,512]{2,1,0:T(8,128)(2,1)}, bf16[4,256,512]{2,1,0:T(8,128)(2,1)S(1)}, u32[]{:S(2)}) copy-start(bf16[4,256,512]{2,1,0:T(8,128)(2,1)S(1)} %collective-permute-done.other_ref) | copy-start | bytes 3145732
  28.7 60.4 %copy-start.5 = (f32[32]{0:T(128)S(1)}, f32[32]{0:T(128)}, u32[]{:S(2)}) copy-start(f32[32]{0:T(128)} %param.9) | copy-start | bytes 388
  28.7 60.5 %copy-start.4 = (bf16[1,4,64]{2,1,0:T(4,128)(2,1)S(1)}, bf16[1,4,64]{2,1,0:T(4,128)(2,1)}, u32[]{:S(2)}) copy-start(bf16[1,4,64]{2,1,0:T(4,128)(2,1)} %param.8) | copy-start | bytes 1540
  82.8 8.9 %copy-start.1 = (bf16[32,96,128]{2,1,0:T(8,128)(2,1)}, bf16[32,96,128]{2,1,0:T(8,128)(2,1)S(1)}, u32[]{:S(2)}) copy-start(bf16[32,96,128]{2,1,0:T(8,128)(2,1)S(1)} %all_to_all.17.mine_ref) | copy-start | bytes 2359300
  82.8 8.2 %collective-permute-start.1 = (bf16[32,96,128]{2,1,0:T(8,128)(2,1)S(1)}, bf16[32,96,128]{2,1,0:T(8,128)(2,1)S(1)}, u32[]{:S(2)}, u32[]{:S(2)}) collective-permute-start(bf16[32,96,128]{2,1,0:T(8,128)(2,1)S(1)} %all_to_all.17.mine_ref), channel_id=1, source_target_pairs={{0,1},{1,0},{2,3},{3,2},{4,5},{5,4},{6,7},{7,6},{8,9},{9,8},{10,11... | collective-permute-start | bytes 2359304 | tf_op jit(solution)/shard_map/ppermute | solution.py:113
  91.0 0.9 copy-start.3

commit v2 on v1

v2 whole, which is shorter than its diff:
```python
import jax
import jax.numpy as jnp
from jax import lax
from jax.experimental import pallas as pl
from jax.experimental.pallas import tpu as pltpu
from jax.sharding import Mesh, PartitionSpec as P

HEAD_DIM = 64
F32, BF16 = jnp.float32, jnp.bfloat16
SMEM = pl.BlockSpec(memory_space=pltpu.SMEM)
VMEM = pl.BlockSpec(memory_space=pltpu.VMEM)
ANY = pl.BlockSpec(memory_space=pl.ANY)


def project_kernel(core_ref, mine_ref, other_ref, w_ref, out_ref):
    core = core_ref[0]
    heads, both, half, _ = out_ref.shape
    seq = pl.program_id(0)
    for ref, which in ((mine_ref, core), (other_ref, 1 - core)):
        rows = jnp.dot(ref[...], w_ref[...], preferred_element_type=F32)
        for h in range(heads):
            part = rows[:, HEAD_DIM * h : HEAD_DIM * h + HEAD_DIM]
            out_ref[h, which * (both // 2) + seq] = jnp.concatenate([part[:half], part[half:]], axis=1).astype(BF16)


def project(core, mine, other, w, seqs, half):
    heads = w.shape[1] // HEAD_DIM
    rows = pl.BlockSpec((2 * half, w.shape[0]), lambda i: (i, 0))
    return pl.pallas_call(
        project_kernel,
        out_shape=jax.ShapeDtypeStruct((heads, 2 * seqs, half, 128), BF16),
        grid=(seqs,),
        in_specs=[SMEM, rows, rows, pl.BlockSpec(w.shape, lambda i: (0, 0))],
        out_specs=pl.BlockSpec((heads, 2 * seqs, half, 128), lambda i: (0, 0, 0, 0)),
        compiler_params=pltpu.CompilerParams(vmem_limit_bytes=24 << 20),
        cost_estimate=pl.CostEstimate(flops=4 * mine.shape[0] * w.shape[0] * w.shape[1], bytes_accessed=8 << 20, transcendentals=0),
    )(core, mine, other, w)


def split3(a):
    hi = a.astype(BF16)
    rest = a - hi.astype(F32)
    mid = rest.astype(BF16)
    return hi, mid, (rest - mid.astype(F32)).astype(BF16)


PARTS = 4


def read_kernel(info_ref, off_ref, mine_ref, other_ref, q_ref, cache_ref, out_ref, kv_ref, sems):
    blocks, half, width = mine_ref.shape
    span = kv_ref.shape[0]
    group = q_ref.shape[1]
    core, first = info_ref[0], info_ref[1]
    swap = core == 1
    piece = span // PARTS
    copies = []
    for b in range(blocks):
        a, o = mine_ref[b], other_ref[b]
        keys = jnp.where(swap, o, a)
        values = jnp.where(swap, a, o)
        base = 2 * half * b
        kv_ref[pl.ds(base, half)] = jnp.concatenate([keys[:, :HEAD_DIM], values[:, :HEAD_DIM]], axis=1)
        kv_ref[pl.ds(base + half, half)] = jnp.concatenate([keys[:, HEAD_DIM:], values[:, HEAD_DIM:]], axis=1)
        done = base + 2 * half
        if done % piece == 0:
            n = done // piece - 1
            copy = pltpu.make_async_copy(
                kv_ref.at[pl.ds(n * piece, piece)], cache_ref.at[0, 0, pl.ds(n * piece, piece)], sems.at[n]
            )
            copy.start()
            copies.append(copy)
    tiles = span // 128
    rows = 8
    q = jnp.concatenate([q_ref[0], jnp.zeros((group, width - HEAD_DIM), BF16)], axis=1)
    q = jnp.concatenate([q, jnp.zeros((rows - group, width), BF16)], axis=0)
    row = lax.broadcasted_iota(jnp.int32, (rows, 128), 0)
    off = jnp.zeros((rows, 128), F32)
    for g in range(group):
        off = jnp.where(row == g, off_ref[first + g], off)
    scores = lax.dot_general(q, kv_ref[...], (((1,), (1,)), ((), ())), preferred_element_type=F32)
    z = scores * (HEAD_DIM ** -0.5) + off[:, :1]
    stay = -(jnp.maximum(z, 0.0) + jnp.log1p(jnp.exp(-jnp.abs(z))))
    stacked = jnp.concatenate([stay[:, 128 * t : 128 * t + 128] for t in range(tiles)], axis=0)
    r = lax.broadcasted_iota(jnp.int32, (128, 128), 0)
    c = lax.broadcasted_iota(jnp.int32, (128, 128), 1)
    from_here = (r >= c).astype(F32).astype(BF16)
    suffix = None
    for part in split3(stacked):
        part = jnp.dot(part, from_here, preferred_element_type=F32)
        suffix = part if suffix is None else suffix + part
    later = jnp.zeros((rows, 1), F32)
    pieces = [None] * tiles
    for t in reversed(range(tiles)):
        own = suffix[rows * t : rows * t + rows]
        pieces[t] = own + later
        later = later + own[:, :1]
    weight = jnp.exp(z + jnp.concatenate(pieces, axis=1)).astype(BF16)
    out = jnp.dot(weight, kv_ref[...], preferred_element_type=F32)
    out_ref[0] = out[:group, HEAD_DIM:].astype(BF16)
    for copy in copies:
        copy.wait()


def read(info, off, mine, other, q):
    blocks, half, width = mine.shape
    span = 2 * blocks * half
    group = q.shape[1]
    return pl.pallas_call(
        read_kernel,
        out_shape=(jax.ShapeDtypeStruct((1, 1, span, width), BF16), jax.ShapeDtypeStruct(q.shape, BF16)),
        in_specs=[SMEM, SMEM, VMEM, VMEM, VMEM],
        out_specs=(ANY, VMEM),
        scratch_shapes=[pltpu.VMEM((span, width), BF16), pltpu.SemaphoreType.DMA((PARTS,))],
        compiler_params=pltpu.CompilerParams(vmem_limit_bytes=24 << 20),
        cost_estimate=pl.CostEstimate(flops=32 * span * width, bytes_accessed=4 << 20, transcendentals=24 * span),
    )(info, off, mine, other, q)


def local(mixer_input, key_weight, content_projection_matrix, new_queries, head_stick_offset):
    seqs, block, width = mixer_input.shape
    depth, columns = key_weight.shape
    half = block // 2
    core = lax.axis_index("core").astype(jnp.int32)
    other = [(0, 1), (1, 0)]
    rows = mixer_input.reshape(seqs * block, width)
    their_rows = lax.ppermute(rows, "core", other)
    chips = lax.axis_size("x")
    weight = jnp.stack([key_weight, content_projection_matrix])
    weight = jnp.broadcast_to(weight, (chips, *weight.shape)).reshape(2 * chips, depth, columns)
    weight = lax.all_to_all(weight, ("x", "core"), 0, 0, tiled=True).reshape(2 * chips * depth, columns)
    packed = project(core.reshape(1), rows, their_rows, weight, seqs, half)
    packed = lax.all_to_all(packed, "x", 0, 0, tiled=True)
    packed = packed.reshape(packed.shape[0] * 2 * seqs, half, 128)
    mine = lax.all_to_all(packed, ("z", "y"), 0, 0, tiled=True)
    theirs = lax.ppermute(mine, "core", other)
    first = (lax.axis_index("x") * 2 + core) * new_queries.shape[1]
    return read(jnp.stack([core, first]), head_stick_offset, mine, theirs, new_queries)


def solution(mesh):
    wide = Mesh(mesh.devices.reshape(2, 4, 8, 4, 2), ("gr", "z", "y", "x", "core"))
    sp, tp = ("z", "y"), ("x", "core")
    return jax.shard_map(
        local,
        mesh=wide,
        in_specs=(P(("gr", *tp), sp, None), P(tp, None), P(tp, None), P(("gr", *sp), tp, None), P()),
        out_specs=(P(("gr", *sp), tp, None, None), P(("gr", *sp), tp, None)),
        check_vma=False,
    )
```

time: 97 us -> 89.6 us (0.924)
  blocking collectives: 64.1 us -> 41.5 us
  waiting for transfers between devices: 3.46 us -> 16.8 us
  starting transfers between devices: 13.7 us -> 19.1 us
  local copies, waits for them, and re-layouts: 5.4 us -> 2.94 us
  Pallas kernels: 8.56 us -> 7.14 us
    all_to_all x3 -> x2, blocking collectives: 64.1 us -> 41.5 us  [the longest x1 27.6 us: local(): mine = lax.all_to_all(packed, ('z', 'y'), 0, 0, tiled=True)]
    all_to_all x0 -> x1, waiting for transfers between devices: none -> 14.9 us  [local(): lax.all_to_all(weight, ('x', 'core'), 0, 0, tiled=True)]
    ppermute x0 -> x1, starting transfers between devices: none -> 8.75 us  [local(): their_rows = lax.ppermute(rows, 'core', other)]
    ppermute x2 -> x1, starting transfers between devices: 13.7 us -> 6.85 us  [local(): theirs = lax.ppermute(mine, 'core', other)]
    all_to_all x0 -> x1, starting transfers between devices: none -> 3.51 us  [local(): lax.all_to_all(weight, ('x', 'core'), 0, 0, tiled=True)]
    ppermute x2 -> x1, waiting for transfers between devices: 3.46 us -> 1.81 us  [local(): theirs = lax.ppermute(mine, 'core', other)]
    unnamed x14 -> x6, local copies, waits for them, and re-layouts: 3.16 us -> 1.9 us
  transfers between devices with their start and end apart: 2 -> 3, of which waited for: 2 -> 2; matrix products, arithmetic and copies ran while one was open for 1% -> 2% of each run, Pallas kernels for 0% -> 0%
where the time goes in v2:
time: 89.6 us; the launch traced here: 89.2 us
  blocking collectives  41.5 us (46%)
  starting transfers between devices  19.1 us (21%)
  waiting for transfers between devices  16.8 us (19%)
  Pallas kernels  7.14 us (8%)
  local copies, waits for them, and re-layouts  2.94 us (3%)
  other arithmetic  1.07 us (1%)
    all_to_all x1, blocking collectives, local(): mine = lax.all_to_all(packed, ('z', 'y'), 0, 0, tiled=True)  27.6 us
    all_to_all x1, waiting for transfers between devices, local(): lax.all_to_all(weight, ('x', 'core'), 0, 0, tiled=True)  14.9 us
    all_to_all x1, blocking collectives, local(): packed = lax.all_to_all(packed, 'x', 0, 0, tiled=True)  13.8 us
    ppermute x1, starting transfers between devices, local(): their_rows = lax.ppermute(rows, 'core', other)  8.75 us
    ppermute x1, starting transfers between devices, local(): theirs = lax.ppermute(mine, 'core', other)  6.85 us
    pallas_call x1, Pallas kernels, project(): pl.pallas_call(project_kernel, out_shape=jax.ShapeDtypeStruct((heads, 2 *...  4.33 us
    all_to_all x1, starting transfers between devices, local(): lax.all_to_all(weight, ('x', 'core'), 0, 0, tiled=True)  3.51 us
    pallas_call x1, Pallas kernels, read(): pl.pallas_call(read_kernel, out_shape=(jax.ShapeDtypeStruct((1, 1, span,...  2.8 us
  transfers between devices with their start and end apart: 3, of which 2 were waited for; matrix products, arithmetic and copies ran while one was open for 2% of the time, Pallas kernels for 0%

profile of v2, /device:TPU:1, one launch (start us, length us, event | category | flops | bytes accessed | tf_op | source)
XLA Modules:
  0.0 89.2 jit_solution(12689038737188495413)
XLA Ops:
  0.6 8.8 %collective-permute-start = (bf16[768,2048]{1,0:T(8,128)(2,1)}, bf16[768,2048]{1,0:T(8,128)(2,1)}, u32[]{:S(2)}, u32[]{:S(2)}) collective-permute-start(bf16[768,2048]{1,0:T(8,128)(2,1)} %bitcast.9), channel_id=1, source_target_pairs={{0,1},{1,0},{2,3},{3,2},{4,5},{5,4},{6,7},{7,6},{8,9},{9,8},{10,11... | collective-permute-start | bytes 9437192 | tf_op jit(solution)/shard_map/ppermute | solution.py:127
  9.4 1.0 %pad_maximum_fusion = bf16[2,256,256]{2,1,0:T(8,128)(2,1)S(1)} fusion(bf16[1,256,256]{2,1,0:T(8,128)(2,1)} %bitcast.12, bf16[1,256,256]{2,1,0:T(8,128)(2,1)} %bitcast.13), kind=kLoop, calls=%fused_computation | loop fusion | flops 131072 | bytes 524288 | tf_op jit(solution)/shard_map/stack | solution.py:129
  10.4 1.0 %broadcast_in_dim.3 = bf16[4,2,256,256]{3,2,1,0:T(8,128)(2,1)} broadcast(bf16[2,256,256]{2,1,0:T(8,128)(2,1)S(1)} %pad_maximum_fusion), dimensions={1,2,3} | broadcast | bytes 1310720 | tf_op jit(solution)/shard_map/broadcast_in_dim | solution.py:130
  11.4 3.5 %all-to-all-start = ((bf16[8,256,256]{2,1,0:T(8,128)(2,1)}), bf16[8,256,256]{2,1,0:T(8,128)(2,1)S(1)}, u32[]{:S(2)}, u32[]{:S(2)}) async-start(bf16[8,256,256]{2,1,0:T(8,128)(2,1)} %bitcast.5), calls=%async_computation | async-start | bytes 2097152 | tf_op jit(solution)/shard_map/all_to_all | solution.py:131
  14.9 14.9 %all-to-all-done = bf16[8,256,256]{2,1,0:T(8,128)(2,1)S(1)} async-done(((bf16[8,256,256]{2,1,0:T(8,128)(2,1)}), bf16[8,256,256]{2,1,0:T(8,128)(2,1)S(1)}, u32[]{:S(2)}, u32[]{:S(2)}) %all-to-all-start) | async-done | bytes 1048608 | tf_op jit(solution)/shard_map/all_to_all | solution.py:131
  29.9 0.0 collective-permute-done.other_ref
  29.9 0.0 copy-start
  29.9 1.9 %copy-done = bf16[4,192,2048]{2,1,0:T(8,128)(2,1)S(1)} copy-done((bf16[4,192,2048]{2,1,0:T(8,128)(2,1)S(1)}, bf16[4,192,2048]{2,1,0:T(8,128)(2,1)}, u32[]{:S(2)}) %copy-start) | copy-done | bytes 3145752
  31.8 4.3 %shard_map.68 = bf16[4,8,96,128]{3,2,1,0:T(8,128)(2,1)S(1)} custom-call(s32[1]{0:T(128)} %bitcast.core_ref, bf16[768,2048]{1,0:T(8,128)(2,1)S(1)} %bitcast.10, bf16[768,2048]{1,0:T(8,128)(2,1)} %collective-permute-done.other_ref, bf16[2048,256]{1,0:T(8,128)(2,1)S(1)} %bitcast.8), custom_call_target="tpu_custom_call" | custom-call | flops 1610612736 | bytes 8388608 | tf_op jit(solution)/shard_map/pallas_call | solution.py:29
  36.1 0.0 copy-start.1
  36.1 0.0 copy-start.2
  36.2 13.8 %all_to_all.15 = bf16[4,8,96,128]{3,2,1,0:T(8,128)(2,1)S(1)} all-to-all(bf16[4,8,96,128]{3,2,1,0:T(8,128)(2,1)S(1)} %shard_map.68), channel_id=1, replica_groups=mesh['gr'=2,'z'=4,'y'=8,'x'=4,'core'=2] {'x'}, dimensions={0} | all-to-all | bytes 1572864 | tf_op jit(solution)/shard_map/all_to_all | solution.py:133
  50.0 27.6 %all_to_all.16.mine_ref = bf16[32,96,128]{2,1,0:T(8,128)(2,1)S(1)} all-to-all(bf16[32,96,128]{2,1,0:T(8,128)(2,1)S(1)} %bitcast.11), channel_id=1, replica_groups=mesh['gr'=2,'z'=4,'y'=8,'x'=4,'core'=2] {'z','y'}, dimensions={0} | all-to-all | bytes 1572864 | tf_op jit(solution)/shard_map/all_to_all | solution.py:135
  77.6 6.9 %collective-permute-start.1 = (bf16[32,96,128]{2,1,0:T(8,128)(2,1)S(1)}, bf16[32,96,128]{2,1,0:T(8,128)(2,1)S(1)}, u32[]{:S(2)}, u32[]{:S(2)}) collective-permute-start(bf16[32,96,128]{2,1,0:T(8,128)(2,1)S(1)} %all_to_all.16.mine_ref), channel_id=1, source_target_pairs={{0,1},{1,0},{2,3},{3,2},{4,5},{5,4},{6,7},{7,6},{8,9},{9,8},{10,11... | collective-permute-start | bytes 2359304 | tf_op jit(solution)/shard_map/ppermute | solution.py:136
  84.5 0.1 pad_add_fusion.info_ref
  84.6 1.8 %collective-permute-done.1.other_ref = bf16[32,96,128]{2,1,0:T(8,128)(2,1)S(1)} collective-permute-done((bf16[32,96,128]{2,1,0:T(8,128)(2,1)S(1)}, bf16[32,96,128]{2,1,0:T(8,128)(2,1)S(1)}, u32[]{:S(2)}, u32[]{:S(2)}) %collective-permute-start.1) | collective-permute-done | bytes 786464 | tf_op jit(solution)/shard_map/ppermute | solution.py:136
  86.4 0.0 copy-done.1
  86.4 0.0 copy-done.2
  86.4 2.8 %shard_map.69 = (bf16[1,1,6144,128]{3,2,1,0:T(8,128)(2,1)}, bf16[1,4,64]{2,1,0:T(4,128)(2,1)}) custom-call(s32[2]{0:T(128)S(1)} %pad_add_fusion.info_ref, f32[32]{0:T(128)S(1)} %copy-done.2, bf16[32,96,128]{2,1,0:T(8,128)(2,1)S(1)} %all_to_all.16.mine_ref, bf16[32,96,128]{2,1,0:T(8,128)(2,1)S(1)} %collective-permute-done.1.other_ref, ...), custom_call_target="tpu_custom_call" | custom-call | flops 25165824 | bytes 4194304 | tf_op jit(solution)/shard_map/pallas_call | solution.py:109
Async XLA Ops:
  0.6 29.3 %collective-permute-start = (bf16[768,2048]{1,0:T(8,128)(2,1)}, bf16[768,2048]{1,0:T(8,128)(2,1)}, u32[]{:S(2)}, u32[]{:S(2)}) collective-permute-start(bf16[768,2048]{1,0:T(8,128)(2,1)} %bitcast.9), channel_id=1, source_target_pairs={{0,1},{1,0},{2,3},{3,2},{4,5},{5,4},{6,7},{7,6},{8,9},{9,8},{10,11... | collective-permute-start | bytes 9437192 | tf_op jit(solution)/shard_map/ppermute | solution.py:127
  11.4 18.5 %all-to-all-start = ((bf16[8,256,256]{2,1,0:T(8,128)(2,1)}), bf16[8,256,256]{2,1,0:T(8,128)(2,1)S(1)}, u32[]{:S(2)}, u32[]{:S(2)}) async-start(bf16[8,256,256]{2,1,0:T(8,128)(2,1)} %bitcast.5), calls=%async_computation | async-start | bytes 2097152 | tf_op jit(solution)/shard_map/all_to_all | solution.py:131
  29.9 1.9 %copy-start = (bf16[4,192,2048]{2,1,0:T(8,128)(2,1)S(1)}, bf16[4,192,2048]{2,1,0:T(8,128)(2,1)}, u32[]{:S(2)}) copy-start(bf16[4,192,2048]{2,1,0:T(8,128)(2,1)} %param.5) | copy-start | bytes 9437188
  36.1 50.2 %copy-start.1 = (bf16[1,4,64]{2,1,0:T(4,128)(2,1)S(1)}, bf16[1,4,64]{2,1,0:T(4,128)(2,1)}, u32[]{:S(2)}) copy-start(bf16[1,4,64]{2,1,0:T(4,128)(2,1)} %q_ref.1) | copy-start | bytes 1540
  36.1 50.2 %copy-start.2 = (f32[32]{0:T(128)S(1)}, f32[32]{0:T(128)}, u32[]{:S(2)}) copy-start(f32[32]{0:T(128)} %off_ref.1) | copy-start | bytes 388
  77.6 8.7 %collective-permute-start.1 = (bf16[32,96,128]{2,1,0:T(8,128)(2,1)S(1)}, bf16[32,96,128]{2,1,0:T(8,128)(2,1)S(1)}, u32[]{:S(2)}, u32[]{:S(2)}) collective-permute-start(bf16[32,96,128]{2,1,0:T(8,128)(2,1)S(1)} %all_to_all.16.mine_ref), channel_id=1, source_target_pairs={{0,1},{1,0},{2,3},{3,2},{4,5},{5,4},{6,7},{7,6},{8,9},{9,8},{10,11... | collective-permute-start | bytes 2359304 | tf_op jit(solution)/shard_map/ppermute | solution.py:136

commit v3 on v2

v3 whole, which is shorter than its diff:
```python
import jax
import jax.numpy as jnp
from jax import lax
from jax.experimental import pallas as pl
from jax.experimental.pallas import tpu as pltpu
from jax.sharding import Mesh, PartitionSpec as P

HEAD_DIM = 64
F32, BF16 = jnp.float32, jnp.bfloat16
SMEM = pl.BlockSpec(memory_space=pltpu.SMEM)
VMEM = pl.BlockSpec(memory_space=pltpu.VMEM)
HBM = pl.BlockSpec(memory_space=pltpu.HBM)
GRANT = pltpu.CompilerParams(vmem_limit_bytes=20 << 20)


def first_kernel(core_ref, x_ref, w_ref, sum_ref, rows_ref, sems):
    core = core_ref[0]
    shards, depth, _ = w_ref.shape
    copies = []
    for which in (core, 1 - core):
        for s in range(shards):
            at = pl.ds(pl.multiple_of((2 * s + which) * depth, depth), depth)
            copy = pltpu.make_async_copy(x_ref.at[:, at], rows_ref.at[:, at], sems.at[len(copies)])
            copy.start()
            copies.append((copy, at))
    total = None
    for s in range(shards):
        copy, at = copies[s]
        copy.wait()
        part = jnp.dot(rows_ref[:, at], w_ref[s], preferred_element_type=F32)
        total = part if total is None else total + part
    sum_ref[...] = total
    for copy, _ in copies[shards:]:
        copy.wait()


def second_kernel(core_ref, rows_ref, w_ref, sum_ref, out_ref):
    core = core_ref[0]
    shards, depth, width = w_ref.shape
    slots, seqs, half, _ = out_ref.shape
    total = sum_ref[...]
    for s in range(shards):
        at = pl.multiple_of((2 * s + 1 - core) * depth, depth)
        total = total + jnp.dot(rows_ref[:, pl.ds(at, depth)], w_ref[s], preferred_element_type=F32)
    rows = total.astype(BF16)
    for slot in range(slots):
        for i in range(seqs):
            start, key = (2 * i + slot % 2) * half, HEAD_DIM * (slot // 2)
            value = key + width // 2
            part = rows[start : start + half]
            out_ref[slot, i] = jnp.concatenate([part[:, key : key + HEAD_DIM], part[:, value : value + HEAD_DIM]], axis=1)


def first(core, x, w):
    shards, depth, width = w.shape
    return pl.pallas_call(
        first_kernel,
        out_shape=(jax.ShapeDtypeStruct((x.shape[0], width), F32), jax.ShapeDtypeStruct(x.shape, BF16)),
        in_specs=[SMEM, HBM, VMEM],
        out_specs=(VMEM, VMEM),
        scratch_shapes=[pltpu.SemaphoreType.DMA((2 * shards,))],
        compiler_params=GRANT,
        cost_estimate=pl.CostEstimate(flops=x.shape[0] * x.shape[1] * width, bytes_accessed=4 << 20, transcendentals=0),
    )(core, x, w)


def second(core, rows, w, total, seqs, half):
    slots = w.shape[2] // HEAD_DIM
    return pl.pallas_call(
        second_kernel,
        out_shape=jax.ShapeDtypeStruct((slots, seqs, half, 2 * HEAD_DIM), BF16),
        in_specs=[SMEM, VMEM, VMEM, VMEM],
        out_specs=VMEM,
        compiler_params=GRANT,
        cost_estimate=pl.CostEstimate(flops=rows.shape[0] * rows.shape[1] * w.shape[2], bytes_accessed=4 << 20, transcendentals=0),
    )(core, rows, w, total)


def split3(a):
    hi = a.astype(BF16)
    rest = a - hi.astype(F32)
    mid = rest.astype(BF16)
    return hi, mid, (rest - mid.astype(F32)).astype(BF16)


def read_kernel(core_ref, first_ref, off_ref, mine_ref, other_ref, q_ref, cache_ref, out_ref, kv_ref, sems):
    blocks, half, width = mine_ref.shape
    span = kv_ref.shape[0]
    group = q_ref.shape[1]
    core, first_head = core_ref[0], first_ref[0]
    copies = []
    for ref, which in ((mine_ref, core), (other_ref, 1 - core)):
        copy = pltpu.make_async_copy(ref, cache_ref.at[:, which], sems.at[len(copies)])
        copy.start()
        copies.append(copy)
    for b in range(blocks):
        base = 2 * half * b
        kv_ref[pl.ds(pl.multiple_of(base + core * half, half), half)] = mine_ref[b]
        kv_ref[pl.ds(pl.multiple_of(base + (1 - core) * half, half), half)] = other_ref[b]
    tiles = span // 128
    rows = 8
    q = jnp.concatenate([q_ref[0], jnp.zeros((group, width - HEAD_DIM), BF16)], axis=1)
    q = jnp.concatenate([q, jnp.zeros((rows - group, width), BF16)], axis=0)
    row = lax.broadcasted_iota(jnp.int32, (rows, 128), 0)
    off = jnp.zeros((rows, 128), F32)
    for g in range(group):
        off = jnp.where(row == g, off_ref[first_head + g], off)
    scores = lax.dot_general(q, kv_ref[...], (((1,), (1,)), ((), ())), preferred_element_type=F32)
    z = scores * (HEAD_DIM ** -0.5) + off[:, :1]
    stay = -(jnp.maximum(z, 0.0) + jnp.log1p(jnp.exp(-jnp.abs(z))))
    stacked = jnp.concatenate([stay[:, 128 * t : 128 * t + 128] for t in range(tiles)], axis=0)
    r = lax.broadcasted_iota(jnp.int32, (128, 128), 0)
    c = lax.broadcasted_iota(jnp.int32, (128, 128), 1)
    from_here = (r >= c).astype(F32).astype(BF16)
    suffix = None
    for part in split3(stacked):
        part = jnp.dot(part, from_here, preferred_element_type=F32)
        suffix = part if suffix is None else suffix + part
    later = jnp.zeros((rows, 1), F32)
    pieces = [None] * tiles
    for t in reversed(range(tiles)):
        own = suffix[rows * t : rows * t + rows]
        pieces[t] = own + later
        later = later + own[:, :1]
    weight = jnp.exp(z + jnp.concatenate(pieces, axis=1)).astype(BF16)
    out = jnp.dot(weight, kv_ref[...], preferred_element_type=F32)
    out_ref[0] = out[:group, HEAD_DIM:].astype(BF16)
    for copy in copies:
        copy.wait()


def read(core, first_head, off, mine, other, q):
    blocks, half, width = mine.shape
    span = 2 * blocks * half
    cache, out = pl.pallas_call(
        read_kernel,
        out_shape=(jax.ShapeDtypeStruct((blocks, 2, half, width), BF16), jax.ShapeDtypeStruct(q.shape, BF16)),
        in_specs=[SMEM, SMEM, SMEM, VMEM, VMEM, VMEM],
        out_specs=(HBM, VMEM),
        scratch_shapes=[pltpu.VMEM((span, width), BF16), pltpu.SemaphoreType.DMA((2,))],
        compiler_params=GRANT,
        cost_estimate=pl.CostEstimate(flops=32 * span * width, bytes_accessed=4 << 20, transcendentals=24 * span),
    )(core, first_head, off, mine, other, q)
    return cache.reshape(1, 1, span, width), out


def local(mixer_input, key_weight, content_projection_matrix, new_queries, head_stick_offset):
    seqs, block, width = mixer_input.shape
    half = block // 2
    core = lax.axis_index("core").astype(jnp.int32)
    core_arg = core.reshape(1)
    first_head = ((lax.axis_index("x") * 2 + core) * new_queries.shape[1]).reshape(1)
    swap = [(0, 1), (1, 0)]
    weight = jnp.concatenate([key_weight, content_projection_matrix], axis=1)
    weight = jnp.broadcast_to(weight, (lax.axis_size("x"), *weight.shape))
    mine = lax.all_to_all(weight, "x", 0, 0, tiled=True)
    theirs = lax.ppermute(mine, "core", swap)
    total, rows = first(core_arg, mixer_input.reshape(seqs * block, width), mine)
    packed = second(core_arg, rows, theirs, total, seqs, half)
    packed = lax.all_to_all(packed, ("x", "core"), 0, 0, tiled=True)
    packed = packed.reshape(packed.shape[0] * seqs, half, 2 * HEAD_DIM)
    mine = lax.all_to_all(packed, ("z", "y"), 0, 0, tiled=True)
    theirs = lax.ppermute(mine, "core", swap)
    return read(core_arg, first_head, head_stick_offset, mine, theirs, new_queries)


def solution(mesh):
    wide = Mesh(mesh.devices.reshape(2, 4, 8, 4, 2), ("gr", "z", "y", "x", "core"))
    sp, tp = ("z", "y"), ("x", "core")
    return jax.shard_map(
        local,
        mesh=wide,
        in_specs=(P(("gr", *tp), sp, None), P(tp, None), P(tp, None), P(("gr", *sp), tp, None), P()),
        out_specs=(P(("gr", *sp), tp, None, None), P(("gr", *sp), tp, None)),
        check_vma=False,
    )
```

time: 89.6 us -> 87.9 us (0.981)
  blocking collectives: 41.5 us -> 62.7 us
  waiting for transfers between devices: 16.8 us -> 1.88 us
  starting transfers between devices: 19.1 us -> 13.7 us
  Pallas kernels: 7.14 us -> 5.62 us
  local copies, waits for them, and re-layouts: 2.94 us -> 1.97 us
    all_to_all x1 -> x2, blocking collectives: 13.8 us -> 29.7 us  [the longest x1 15.2 us: local(): mine = lax.all_to_all(weight, 'x', 0, 0, tiled=True)]
    all_to_all x1 -> x0, waiting for transfers between devices: 14.9 us -> none  [local(): lax.all_to_all(weight, ('x', 'core'), 0, 0, tiled=True)]
    all_to_all x1, blocking collectives: 27.6 us -> 32.9 us  [local(): mine = lax.all_to_all(packed, ('z', 'y'), 0, 0, tiled=True)]
    all_to_all x1 -> x0, starting transfers between devices: 3.51 us -> none  [local(): lax.all_to_all(weight, ('x', 'core'), 0, 0, tiled=True)]
    ppermute x2, starting transfers between devices: 15.6 us -> 13.7 us  [local(): theirs = lax.ppermute(mine, 'core', swap)]
    pallas_call x2 -> x3, Pallas kernels: 7.14 us -> 5.62 us  [the longest x1 2.56 us: read(): pl.pallas_call(read_kernel, out_shape=(jax.ShapeDtypeStruct((blocks, 2, h...]
    another operation x2 -> x0, other arithmetic: 1.07 us -> none  [the longest x1 0.99 us: local(): weight = jnp.stack([key_weight, content_projection_matrix])]
    concatenate x0 -> x1, other arithmetic: none -> 0.99 us  [local(): weight = jnp.concatenate([key_weight, content_projection_matrix], axis=1)]
  transfers between devices with their start and end apart: 3 -> 2, of which waited for: 2 -> 1; matrix products, arithmetic and copies ran while one was open for 2% -> 0% of each run, Pallas kernels for 0% -> 2%
where the time goes in v3:
time: 87.9 us; the launch traced here: 87.5 us
  blocking collectives  62.7 us (71%)
  starting transfers between devices  13.7 us (16%)
  Pallas kernels  5.62 us (6%)
  local copies, waits for them, and re-layouts  1.97 us (2%)
  waiting for transfers between devices  1.88 us (2%)
  other arithmetic  0.99 us (1%)
    all_to_all x1, blocking collectives, local(): mine = lax.all_to_all(packed, ('z', 'y'), 0, 0, tiled=True)  32.9 us
    all_to_all x1, blocking collectives, local(): mine = lax.all_to_all(weight, 'x', 0, 0, tiled=True)  15.2 us
    all_to_all x1, blocking collectives, local(): packed = lax.all_to_all(packed, ('x', 'core'), 0, 0, tiled=True)  14.5 us
    ppermute x2, starting transfers between devices, local(): theirs = lax.ppermute(mine, 'core', swap)  13.7 us
    pallas_call x1, Pallas kernels, read(): pl.pallas_call(read_kernel, out_shape=(jax.ShapeDtypeStruct((blocks, 2, h...  2.56 us
    pallas_call x1, Pallas kernels, first(): pl.pallas_call(first_kernel, out_shape=(jax.ShapeDtypeStruct((x.shape[0],...  1.98 us
    unnamed x6, local copies, waits for them, and re-layouts  1.9 us
    ppermute x2, waiting for transfers between devices, local(): theirs = lax.ppermute(mine, 'core', swap)  1.88 us
  transfers between devices with their start and end apart: 2, of which 1 were waited for; matrix products, arithmetic and copies ran while one was open for 0% of the time, Pallas kernels for 2%

profile of v3, /device:TPU:1, one launch (start us, length us, event | category | flops | bytes accessed | tf_op | source)
XLA Modules:
  0.0 87.5 jit_solution(10965079134857274368)
XLA Ops:
  0.6 1.0 %pad_maximum_fusion = bf16[256,512]{1,0:T(8,128)(2,1)S(1)} fusion(bf16[256,256]{1,0:T(8,128)(2,1)} %param.7, bf16[256,256]{1,0:T(8,128)(2,1)} %param.6), kind=kLoop, calls=%fused_computation | loop fusion | flops 524288 | bytes 524288 | tf_op jit(solution)/shard_map/concatenate | solution.py:154
  1.6 0.1 broadcast_in_dim.3
  1.7 15.2 %all_to_all.15.w_ref = bf16[4,256,512]{2,1,0:T(8,128)(2,1)S(1)} all-to-all(bf16[4,256,512]{2,1,0:T(8,128)(2,1)S(1)} %broadcast_in_dim.3), channel_id=1, replica_groups=mesh['gr'=2,'z'=4,'y'=8,'x'=4,'core'=2] {'x'}, dimensions={0} | all-to-all | bytes 2097152 | tf_op jit(solution)/shard_map/all_to_all | solution.py:156
  16.9 7.4 %collective-permute-start = (bf16[4,256,512]{2,1,0:T(8,128)(2,1)S(1)}, bf16[4,256,512]{2,1,0:T(8,128)(2,1)S(1)}, u32[]{:S(2)}, u32[]{:S(2)}) collective-permute-start(bf16[4,256,512]{2,1,0:T(8,128)(2,1)S(1)} %all_to_all.15.w_ref), channel_id=1, source_target_pairs={{0,1},{1,0},{2,3},{3,2},{4,5},{5,4},{6,7},{7,6},{8,9},{9,8},{10,11... | collective-permute-start | bytes 3145736 | tf_op jit(solution)/shard_map/ppermute | solution.py:157
  24.3 0.0 copy-start
  24.3 1.9 %copy-done = bf16[4,192,2048]{2,1,0:T(8,128)(2,1)S(1)} copy-done((bf16[4,192,2048]{2,1,0:T(8,128)(2,1)S(1)}, bf16[4,192,2048]{2,1,0:T(8,128)(2,1)}, u32[]{:S(2)}) %copy-start) | copy-done | bytes 3145752
  26.2 2.0 %shard_map.68 = (f32[768,512]{1,0:T(8,128)S(1)}, bf16[768,2048]{1,0:T(8,128)(2,1)S(1)}) custom-call(s32[1]{0:T(128)} %bitcast.core_ref, bf16[768,2048]{1,0:T(8,128)(2,1)S(1)} %bitcast.5, bf16[4,256,512]{2,1,0:T(8,128)(2,1)S(1)} %all_to_all.15.w_ref), custom_call_target="tpu_custom_call" | custom-call | flops 805306368 | bytes 4194304 | tf_op jit(solution)/shard_map/pallas_call | solution.py:56
  28.2 0.0 collective-permute-done.w_ref
  28.2 1.1 %shard_map.69 = bf16[8,4,96,128]{3,2,1,0:T(8,128)(2,1)S(1)} custom-call(s32[1]{0:T(128)} %bitcast.core_ref, bf16[768,2048]{1,0:T(8,128)(2,1)S(1)} %get-tuple-element.6.rows_ref, bf16[4,256,512]{2,1,0:T(8,128)(2,1)S(1)} %collective-permute-done.w_ref, f32[768,512]{1,0:T(8,128)S(1)} %get-tuple-element.7.sum_ref), custom_call_target="tpu_custom_call" | custom-call | flops 805306368 | bytes 4194304 | tf_op jit(solution)/shard_map/pallas_call | solution.py:69
  29.3 0.0 copy-start.1
  29.3 0.0 copy-start.2
  29.3 14.5 %all_to_all.16 = bf16[8,4,96,128]{3,2,1,0:T(8,128)(2,1)S(1)} all-to-all(bf16[8,4,96,128]{3,2,1,0:T(8,128)(2,1)S(1)} %shard_map.69), channel_id=1, replica_groups=mesh['gr'=2,'z'=4,'y'=8,'x'=4,'core'=2] {'x','core'}, dimensions={0} | all-to-all | bytes 1572864 | tf_op jit(solution)/shard_map/all_to_all | solution.py:160
  43.8 32.9 %all_to_all.17.mine_ref = bf16[32,96,128]{2,1,0:T(8,128)(2,1)S(1)} all-to-all(bf16[32,96,128]{2,1,0:T(8,128)(2,1)S(1)} %bitcast.6), channel_id=1, replica_groups=mesh['gr'=2,'z'=4,'y'=8,'x'=4,'core'=2] {'z','y'}, dimensions={0} | all-to-all | bytes 1572864 | tf_op jit(solution)/shard_map/all_to_all | solution.py:162
  76.8 6.3 %collective-permute-start.1 = (bf16[32,96,128]{2,1,0:T(8,128)(2,1)S(1)}, bf16[32,96,128]{2,1,0:T(8,128)(2,1)S(1)}, u32[]{:S(2)}, u32[]{:S(2)}) collective-permute-start(bf16[32,96,128]{2,1,0:T(8,128)(2,1)S(1)} %all_to_all.17.mine_ref), channel_id=1, source_target_pairs={{0,1},{1,0},{2,3},{3,2},{4,5},{5,4},{6,7},{7,6},{8,9},{9,8},{10,11... | collective-permute-start | bytes 2359304 | tf_op jit(solution)/shard_map/ppermute | solution.py:163
  83.1 1.9 %collective-permute-done.1.other_ref = bf16[32,96,128]{2,1,0:T(8,128)(2,1)S(1)} collective-permute-done((bf16[32,96,128]{2,1,0:T(8,128)(2,1)S(1)}, bf16[32,96,128]{2,1,0:T(8,128)(2,1)S(1)}, u32[]{:S(2)}, u32[]{:S(2)}) %collective-permute-start.1) | collective-permute-done | bytes 786464 | tf_op jit(solution)/shard_map/ppermute | solution.py:163
  85.0 0.0 copy-done.1
  85.0 0.0 copy-done.2
  85.0 2.6 %shard_map.70 = (bf16[32,2,96,128]{3,2,1,0:T(8,128)(2,1)}, bf16[1,4,64]{2,1,0:T(4,128)(2,1)}) custom-call(s32[1]{0:T(128)} %bitcast.core_ref, s32[1]{0:T(128)} %bitcast.1.first_ref, f32[32]{0:T(128)S(1)} %copy-done.2, bf16[32,96,128]{2,1,0:T(8,128)(2,1)S(1)} %all_to_all.17.mine_ref, bf16[32,96,128]{2,1,0:T(8,128)(2,1)S(1)} %collective-permute-done.1.other_ref, ...), custom_call_target="tpu_custom_call" | custom-call | flops 25165824 | bytes 4194304 | tf_op jit(solution)/shard_map/pallas_call | solution.py:135
Async XLA Ops:
  16.9 11.3 %collective-permute-start = (bf16[4,256,512]{2,1,0:T(8,128)(2,1)S(1)}, bf16[4,256,512]{2,1,0:T(8,128)(2,1)S(1)}, u32[]{:S(2)}, u32[]{:S(2)}) collective-permute-start(bf16[4,256,512]{2,1,0:T(8,128)(2,1)S(1)} %all_to_all.15.w_ref), channel_id=1, source_target_pairs={{0,1},{1,0},{2,3},{3,2},{4,5},{5,4},{6,7},{7,6},{8,9},{9,8},{10,11... | collective-permute-start | bytes 3145736 | tf_op jit(solution)/shard_map/ppermute | solution.py:157
  24.3 1.9 %copy-start = (bf16[4,192,2048]{2,1,0:T(8,128)(2,1)S(1)}, bf16[4,192,2048]{2,1,0:T(8,128)(2,1)}, u32[]{:S(2)}) copy-start(bf16[4,192,2048]{2,1,0:T(8,128)(2,1)} %param.5) | copy-start | bytes 9437188
  29.3 55.7 %copy-start.1 = (bf16[1,4,64]{2,1,0:T(4,128)(2,1)S(1)}, bf16[1,4,64]{2,1,0:T(4,128)(2,1)}, u32[]{:S(2)}) copy-start(bf16[1,4,64]{2,1,0:T(4,128)(2,1)} %q_ref.1) | copy-start | bytes 1540
  29.3 55.7 %copy-start.2 = (f32[32]{0:T(128)S(1)}, f32[32]{0:T(128)}, u32[]{:S(2)}) copy-start(f32[32]{0:T(128)} %off_ref.1) | copy-start | bytes 388
  76.8 8.2 %collective-permute-start.1 = (bf16[32,96,128]{2,1,0:T(8,128)(2,1)S(1)}, bf16[32,96,128]{2,1,0:T(8,128)(2,1)S(1)}, u32[]{:S(2)}, u32[]{:S(2)}) collective-permute-start(bf16[32,96,128]{2,1,0:T(8,128)(2,1)S(1)} %all_to_all.17.mine_ref), channel_id=1, source_target_pairs={{0,1},{1,0},{2,3},{3,2},{4,5},{5,4},{6,7},{7,6},{8,9},{9,8},{10,11... | collective-permute-start | bytes 2359304 | tf_op jit(solution)/shard_map/ppermute | solution.py:163

commit v4 on v2

--- a/solution.py
+++ b/solution.py
@@ -5,34 +5,67 @@
 from jax.experimental.pallas import tpu as pltpu
 from jax.sharding import Mesh, PartitionSpec as P
 
+
 HEAD_DIM = 64
 F32, BF16 = jnp.float32, jnp.bfloat16
 SMEM = pl.BlockSpec(memory_space=pltpu.SMEM)
 VMEM = pl.BlockSpec(memory_space=pltpu.VMEM)
-ANY = pl.BlockSpec(memory_space=pl.ANY)
+HBM = pl.BlockSpec(memory_space=pltpu.HBM)
+GRANT = pltpu.CompilerParams(vmem_limit_bytes=16 << 20)
 
 
-def project_kernel(core_ref, mine_ref, other_ref, w_ref, out_ref):
+def stage_kernel(x_ref, out_ref, sem):
+    copy = pltpu.make_async_copy(x_ref, out_ref, sem)
+    copy.start()
+    copy.wait()
+
+
+def stage(x):
+    return pl.pallas_call(
+        stage_kernel,
+        out_shape=jax.ShapeDtypeStruct(x.shape, x.dtype),
+        in_specs=[HBM],
+        out_specs=VMEM,
+        scratch_shapes=[pltpu.SemaphoreType.DMA],
+        compiler_params=GRANT,
+        cost_estimate=pl.CostEstimate(flops=1 << 30, bytes_accessed=6 << 20, transcendentals=0),
+    )(x)
+
+
+CHUNKS = 4
+
+
+def project_kernel(core_ref, mine_ref, other_hbm, w_hbm, out_ref, other_ref, w_ref, sems):
     core = core_ref[0]
     heads, both, half, _ = out_ref.shape
-    seq = pl.program_id(0)
-    for ref, which in ((mine_ref, core), (other_ref, 1 - core)):
-        rows = jnp.dot(ref[...], w_ref[...], preferred_element_type=F32)
-        for h in range(heads):
-            part = rows[:, HEAD_DIM * h : HEAD_DIM * h + HEAD_DIM]
-            out_ref[h, which * (both // 2) + seq] = jnp.concatenate([part[:half], part[half:]], axis=1).astype(BF16)
+    seqs = both // 2
+    depth = w_ref.shape[0] // CHUNKS
+    cuts = [pl.ds(k * depth, depth) for k in range(CHUNKS)]
+    weights = [pltpu.make_async_copy(w_hbm.at[c], w_ref.at[c], sems.at[0, k]) for k, c in enumerate(cuts)]
+    others = [pltpu.make_async_copy(other_hbm.at[:, c], other_ref.at[:, c], sems.at[1, k]) for k, c in enumerate(cuts)]
+    for copy in weights + others:
+        copy.start()
+    for ref, which, copies in ((mine_ref, core, weights), (other_ref, 1 - core, others)):
+        rows = None
+        for c, copy in zip(cuts, copies):
+            copy.wait()
+            part = jnp.dot(ref[:, c], w_ref[c], preferred_element_type=F32)
+            rows = part if rows is None else rows + part
+        for i in range(seqs):
+            for h in range(heads):
+                part = rows[2 * half * i : 2 * half * (i + 1), HEAD_DIM * h : HEAD_DIM * h + HEAD_DIM]
+                out_ref[h, which * seqs + i] = jnp.concatenate([part[:half], part[half:]], axis=1).astype(BF16)
 
 
 def project(core, mine, other, w, seqs, half):
     heads = w.shape[1] // HEAD_DIM
-    rows = pl.BlockSpec((2 * half, w.shape[0]), lambda i: (i, 0))
     return pl.pallas_call(
         project_kernel,
         out_shape=jax.ShapeDtypeStruct((heads, 2 * seqs, half, 128), BF16),
-        grid=(seqs,),
-        in_specs=[SMEM, rows, rows, pl.BlockSpec(w.shape, lambda i: (0, 0))],
-        out_specs=pl.BlockSpec((heads, 2 * seqs, half, 128), lambda i: (0, 0, 0, 0)),
-        compiler_params=pltpu.CompilerParams(vmem_limit_bytes=24 << 20),
+        in_specs=[SMEM, VMEM, HBM, HBM],
+        out_specs=VMEM,
+        scratch_shapes=[pltpu.VMEM(other.shape, BF16), pltpu.VMEM(w.shape, BF16), pltpu.SemaphoreType.DMA((2, CHUNKS))],
+        compiler_params=GRANT,
         cost_estimate=pl.CostEstimate(flops=4 * mine.shape[0] * w.shape[0] * w.shape[1], bytes_accessed=8 << 20, transcendentals=0),
     )(core, mine, other, w)
 
@@ -105,14 +138,13 @@
 def read(info, off, mine, other, q):
     blocks, half, width = mine.shape
     span = 2 * blocks * half
-    group = q.shape[1]
     return pl.pallas_call(
         read_kernel,
         out_shape=(jax.ShapeDtypeStruct((1, 1, span, width), BF16), jax.ShapeDtypeStruct(q.shape, BF16)),
         in_specs=[SMEM, SMEM, VMEM, VMEM, VMEM],
-        out_specs=(ANY, VMEM),
+        out_specs=(HBM, VMEM),
         scratch_shapes=[pltpu.VMEM((span, width), BF16), pltpu.SemaphoreType.DMA((PARTS,))],
-        compiler_params=pltpu.CompilerParams(vmem_limit_bytes=24 << 20),
+        compiler_params=GRANT,
         cost_estimate=pl.CostEstimate(flops=32 * span * width, bytes_accessed=4 << 20, transcendentals=24 * span),
     )(info, off, mine, other, q)
 
@@ -123,12 +155,12 @@
     half = block // 2
     core = lax.axis_index("core").astype(jnp.int32)
     other = [(0, 1), (1, 0)]
-    rows = mixer_input.reshape(seqs * block, width)
-    their_rows = lax.ppermute(rows, "core", other)
     chips = lax.axis_size("x")
     weight = jnp.stack([key_weight, content_projection_matrix])
     weight = jnp.broadcast_to(weight, (chips, *weight.shape)).reshape(2 * chips, depth, columns)
     weight = lax.all_to_all(weight, ("x", "core"), 0, 0, tiled=True).reshape(2 * chips * depth, columns)
+    rows = stage(mixer_input.reshape(seqs * block, width))
+    their_rows = lax.ppermute(rows, "core", other)
     packed = project(core.reshape(1), rows, their_rows, weight, seqs, half)
     packed = lax.all_to_all(packed, "x", 0, 0, tiled=True)
     packed = packed.reshape(packed.shape[0] * 2 * seqs, half, 128)

time: 89.6 us -> 89.6 us (level)
  other arithmetic: 1.07 us -> 0.1 us
  Pallas kernels: 7.14 us -> 8.07 us
    another operation x1, other arithmetic: 0.99 us -> 0.03 us  [local(): weight = jnp.stack([key_weight, content_projection_matrix])]
    unnamed x6 -> x10, local copies, waits for them, and re-layouts: 1.9 us -> 1.9 us
  transfers between devices with their start and end apart: 3 -> 3, of which waited for: 2 -> 2; matrix products, arithmetic and copies ran while one was open for 2% -> 1% of each run, Pallas kernels for 0% -> 0%
where the time goes in v4:
time: 89.6 us; the launch traced here: 89.3 us
  blocking collectives  40.8 us (46%)
  starting transfers between devices  19.8 us (22%)
  waiting for transfers between devices  16.8 us (19%)
  Pallas kernels  8.07 us (9%)
  local copies, waits for them, and re-layouts  2.94 us (3%)
    all_to_all x1, blocking collectives, local(): mine = lax.all_to_all(packed, ('z', 'y'), 0, 0, tiled=True)  27 us
    all_to_all x1, waiting for transfers between devices, local(): lax.all_to_all(weight, ('x', 'core'), 0, 0, tiled=True)  15 us
    all_to_all x1, blocking collectives, local(): packed = lax.all_to_all(packed, 'x', 0, 0, tiled=True)  13.8 us
    ppermute x1, starting transfers between devices, local(): their_rows = lax.ppermute(rows, 'core', other)  8.75 us
    ppermute x1, starting transfers between devices, local(): theirs = lax.ppermute(mine, 'core', other)  6.85 us
    pallas_call x1, Pallas kernels, project(): pl.pallas_call(project_kernel, out_shape=jax.ShapeDtypeStruct((heads, 2 *...  5.01 us
    all_to_all x1, starting transfers between devices, local(): lax.all_to_all(weight, ('x', 'core'), 0, 0, tiled=True)  4.21 us
    pallas_call x1, Pallas kernels, read(): pl.pallas_call(read_kernel, out_shape=(jax.ShapeDtypeStruct((1, 1, span,...  2.85 us
  transfers between devices with their start and end apart: 3, of which 2 were waited for; matrix products, arithmetic and copies ran while one was open for 1% of the time, Pallas kernels for 0%

profile of v4, /device:TPU:1, one launch (start us, length us, event | category | flops | bytes accessed | tf_op | source)
XLA Modules:
  0.0 89.3 jit_solution(8984899415752854042)
XLA Ops:
  0.6 0.0 copy-start
  0.6 1.9 %copy-done = bf16[4,192,2048]{2,1,0:T(8,128)(2,1)S(1)} copy-done((bf16[4,192,2048]{2,1,0:T(8,128)(2,1)S(1)}, bf16[4,192,2048]{2,1,0:T(8,128)(2,1)}, u32[]{:S(2)}) %copy-start) | copy-done | bytes 3145752
  2.5 0.0 copy-start.3
  2.5 0.0 copy-start.4
  2.5 0.2 shard_map.68.mine_ref
  2.8 8.7 %collective-permute-start = (bf16[768,2048]{1,0:T(8,128)(2,1)S(1)}, bf16[768,2048]{1,0:T(8,128)(2,1)}, u32[]{:S(2)}, u32[]{:S(2)}) collective-permute-start(bf16[768,2048]{1,0:T(8,128)(2,1)S(1)} %shard_map.68.mine_ref), channel_id=1, source_target_pairs={{0,1},{1,0},{2,3},{3,2},{4,5},{5,4},{6,7},{7,6},{8,9},{9,8},{10,11... | collective-permute-start | bytes 9437192 | tf_op jit(solution)/shard_map/ppermute | solution.py:163
  11.5 0.0 copy-done.3
  11.5 0.0 copy-done.4
  11.6 1.0 %broadcast_in_dim.3 = bf16[4,2,256,256]{3,2,1,0:T(8,128)(2,1)} broadcast(bf16[2,256,256]{2,1,0:T(8,128)(2,1)S(1)} %pad_maximum_fusion), dimensions={1,2,3} | broadcast | bytes 1310720 | tf_op jit(solution)/shard_map/broadcast_in_dim | solution.py:160
  12.6 4.2 %all-to-all-start = ((bf16[8,256,256]{2,1,0:T(8,128)(2,1)}), bf16[8,256,256]{2,1,0:T(8,128)(2,1)}, u32[]{:S(2)}, u32[]{:S(2)}) async-start(bf16[8,256,256]{2,1,0:T(8,128)(2,1)} %bitcast.9), calls=%async_computation | async-start | bytes 2097152 | tf_op jit(solution)/shard_map/all_to_all | solution.py:161
  16.8 15.0 %all-to-all-done = bf16[8,256,256]{2,1,0:T(8,128)(2,1)} async-done(((bf16[8,256,256]{2,1,0:T(8,128)(2,1)}), bf16[8,256,256]{2,1,0:T(8,128)(2,1)}, u32[]{:S(2)}, u32[]{:S(2)}) %all-to-all-start) | async-done | bytes 1048608 | tf_op jit(solution)/shard_map/all_to_all | solution.py:161
  31.8 0.0 collective-permute-done.other_hbm
  31.8 5.0 %shard_map.69 = bf16[4,8,96,128]{3,2,1,0:T(8,128)(2,1)S(1)} custom-call(s32[1]{0:T(128)} %bitcast.core_ref, bf16[768,2048]{1,0:T(8,128)(2,1)S(1)} %shard_map.68.mine_ref, bf16[768,2048]{1,0:T(8,128)(2,1)} %collective-permute-done.other_hbm, bf16[2048,256]{1,0:T(8,128)(2,1)} %bitcast.6.w_hbm), custom_call_target="tpu_custom_call" | custom-call | flops 1610612736 | bytes 8388608 | tf_op jit(solution)/shard_map/pallas_call | solution.py:62
  36.8 0.0 copy-start.1
  36.9 0.0 copy-start.2
  36.9 13.8 %all_to_all.15 = bf16[4,8,96,128]{3,2,1,0:T(8,128)(2,1)S(1)} all-to-all(bf16[4,8,96,128]{3,2,1,0:T(8,128)(2,1)S(1)} %shard_map.69), channel_id=1, replica_groups=mesh['gr'=2,'z'=4,'y'=8,'x'=4,'core'=2] {'x'}, dimensions={0} | all-to-all | bytes 1572864 | tf_op jit(solution)/shard_map/all_to_all | solution.py:165
  50.7 27.0 %all_to_all.16.mine_ref = bf16[32,96,128]{2,1,0:T(8,128)(2,1)S(1)} all-to-all(bf16[32,96,128]{2,1,0:T(8,128)(2,1)S(1)} %bitcast.10), channel_id=1, replica_groups=mesh['gr'=2,'z'=4,'y'=8,'x'=4,'core'=2] {'z','y'}, dimensions={0} | all-to-all | bytes 1572864 | tf_op jit(solution)/shard_map/all_to_all | solution.py:167
  77.7 6.9 %collective-permute-start.1 = (bf16[32,96,128]{2,1,0:T(8,128)(2,1)S(1)}, bf16[32,96,128]{2,1,0:T(8,128)(2,1)S(1)}, u32[]{:S(2)}, u32[]{:S(2)}) collective-permute-start(bf16[32,96,128]{2,1,0:T(8,128)(2,1)S(1)} %all_to_all.16.mine_ref), channel_id=1, source_target_pairs={{0,1},{1,0},{2,3},{3,2},{4,5},{5,4},{6,7},{7,6},{8,9},{9,8},{10,11... | collective-permute-start | bytes 2359304 | tf_op jit(solution)/shard_map/ppermute | solution.py:168
  84.5 0.1 pad_add_fusion.info_ref
  84.6 1.8 %collective-permute-done.1.other_ref = bf16[32,96,128]{2,1,0:T(8,128)(2,1)S(1)} collective-permute-done((bf16[32,96,128]{2,1,0:T(8,128)(2,1)S(1)}, bf16[32,96,128]{2,1,0:T(8,128)(2,1)S(1)}, u32[]{:S(2)}, u32[]{:S(2)}) %collective-permute-start.1) | collective-permute-done | bytes 786464 | tf_op jit(solution)/shard_map/ppermute | solution.py:168
  86.4 0.0 copy-done.1
  86.4 0.0 copy-done.2
  86.4 2.8 %shard_map.70 = (bf16[1,1,6144,128]{3,2,1,0:T(8,128)(2,1)}, bf16[1,4,64]{2,1,0:T(4,128)(2,1)}) custom-call(s32[2]{0:T(128)S(1)} %pad_add_fusion.info_ref, f32[32]{0:T(128)S(1)} %copy-done.2, bf16[32,96,128]{2,1,0:T(8,128)(2,1)S(1)} %all_to_all.16.mine_ref, bf16[32,96,128]{2,1,0:T(8,128)(2,1)S(1)} %collective-permute-done.1.other_ref, ...), custom_call_target="tpu_custom_call" | custom-call | flops 25165824 | bytes 4194304 | tf_op jit(solution)/shard_map/pallas_call | solution.py:141
  (1 shorter events, 0.0 us)
Async XLA Ops:
  0.6 1.9 %copy-start = (bf16[4,192,2048]{2,1,0:T(8,128)(2,1)S(1)}, bf16[4,192,2048]{2,1,0:T(8,128)(2,1)}, u32[]{:S(2)}) copy-start(bf16[4,192,2048]{2,1,0:T(8,128)(2,1)} %param.5) | copy-start | bytes 9437188
  2.5 9.0 %copy-start.3 = (bf16[256,256]{1,0:T(8,128)(2,1)S(1)}, bf16[256,256]{1,0:T(8,128)(2,1)}, u32[]{:S(2)}) copy-start(bf16[256,256]{1,0:T(8,128)(2,1)} %param.7) | copy-start | bytes 393220
  2.5 9.0 %copy-start.4 = (bf16[256,256]{1,0:T(8,128)(2,1)S(1)}, bf16[256,256]{1,0:T(8,128)(2,1)}, u32[]{:S(2)}) copy-start(bf16[256,256]{1,0:T(8,128)(2,1)} %param.6) | copy-start | bytes 393220
  2.8 29.1 %collective-permute-start = (bf16[768,2048]{1,0:T(8,128)(2,1)S(1)}, bf16[768,2048]{1,0:T(8,128)(2,1)}, u32[]{:S(2)}, u32[]{:S(2)}) collective-permute-start(bf16[768,2048]{1,0:T(8,128)(2,1)S(1)} %shard_map.68.mine_ref), channel_id=1, source_target_pairs={{0,1},{1,0},{2,3},{3,2},{4,5},{5,4},{6,7},{7,6},{8,9},{9,8},{10,11... | collective-permute-start | bytes 9437192 | tf_op jit(solution)/shard_map/ppermute | solution.py:163
  12.6 19.2 %all-to-all-start = ((bf16[8,256,256]{2,1,0:T(8,128)(2,1)}), bf16[8,256,256]{2,1,0:T(8,128)(2,1)}, u32[]{:S(2)}, u32[]{:S(2)}) async-start(bf16[8,256,256]{2,1,0:T(8,128)(2,1)} %bitcast.9), calls=%async_computation | async-start | bytes 2097152 | tf_op jit(solution)/shard_map/all_to_all | solution.py:161
  36.8 49.6 %copy-start.1 = (bf16[1,4,64]{2,1,0:T(4,128)(2,1)S(1)}, bf16[1,4,64]{2,1,0:T(4,128)(2,1)}, u32[]{:S(2)}) copy-start(bf16[1,4,64]{2,1,0:T(4,128)(2,1)} %q_ref.1) | copy-start | bytes 1540
  36.9 49.6 %copy-start.2 = (f32[32]{0:T(128)S(1)}, f32[32]{0:T(128)}, u32[]{:S(2)}) copy-start(f32[32]{0:T(128)} %off_ref.1) | copy-start | bytes 388
  77.7 8.7 %collective-permute-start.1 = (bf16[32,96,128]{2,1,0:T(8,128)(2,1)S(1)}, bf16[32,96,128]{2,1,0:T(8,128)(2,1)S(1)}, u32[]{:S(2)}, u32[]{:S(2)}) collective-permute-start(bf16[32,96,128]{2,1,0:T(8,128)(2,1)S(1)} %all_to_all.16.mine_ref), channel_id=1, source_target_pairs={{0,1},{1,0},{2,3},{3,2},{4,5},{5,4},{6,7},{7,6},{8,9},{9,8},{10,11... | collective-permute-start | bytes 2359304 | tf_op jit(solution)/shard_map/ppermute | solution.py:168

commit v5 on v4

--- a/solution.py
+++ b/solution.py
@@ -32,6 +32,36 @@
     )(x)
 
 
+def spread_kernel(key_ref, value_ref, out_ref, held_ref, in_sems, out_sems):
+    incoming = [pltpu.make_async_copy(ref, held_ref.at[n], in_sems.at[n]) for n, ref in enumerate((key_ref, value_ref))]
+    for copy in incoming:
+        copy.start()
+    outgoing = []
+    for n, copy in enumerate(incoming):
+        copy.wait()
+        for chip in range(out_ref.shape[0] // 2):
+            out = pltpu.make_async_copy(held_ref.at[n], out_ref.at[2 * chip + n], out_sems.at[2 * chip + n])
+            out.start()
+            outgoing.append(out)
+    for copy in outgoing:
+        copy.wait()
+
+
+def spread(key, value, chips):
+    return pl.pallas_call(
+        spread_kernel,
+        out_shape=jax.ShapeDtypeStruct((2 * chips, *key.shape), key.dtype),
+        in_specs=[HBM, HBM],
+        out_specs=HBM,
+        scratch_shapes=[
+            pltpu.VMEM((2, *key.shape), key.dtype),
+            pltpu.SemaphoreType.DMA((2,)),
+            pltpu.SemaphoreType.DMA((2 * chips,)),
+        ],
+        cost_estimate=pl.CostEstimate(flops=1 << 20, bytes_accessed=2 << 20, transcendentals=0),
+    )(key, value)
+
+
 CHUNKS = 4
 
 
@@ -43,12 +73,17 @@
     cuts = [pl.ds(k * depth, depth) for k in range(CHUNKS)]
     weights = [pltpu.make_async_copy(w_hbm.at[c], w_ref.at[c], sems.at[0, k]) for k, c in enumerate(cuts)]
     others = [pltpu.make_async_copy(other_hbm.at[:, c], other_ref.at[:, c], sems.at[1, k]) for k, c in enumerate(cuts)]
-    for copy in weights + others:
+    for copy in weights:
         copy.start()
-    for ref, which, copies in ((mine_ref, core, weights), (other_ref, 1 - core, others)):
+    for copy in weights:
+        copy.wait()
+    for copy in others:
+        copy.start()
+    for ref, which, copies in ((mine_ref, core, None), (other_ref, 1 - core, others)):
         rows = None
-        for c, copy in zip(cuts, copies):
-            copy.wait()
+        for k, c in enumerate(cuts):
+            if copies is not None:
+                copies[k].wait()
             part = jnp.dot(ref[:, c], w_ref[c], preferred_element_type=F32)
             rows = part if rows is None else rows + part
         for i in range(seqs):
@@ -156,8 +191,7 @@
     core = lax.axis_index("core").astype(jnp.int32)
     other = [(0, 1), (1, 0)]
     chips = lax.axis_size("x")
-    weight = jnp.stack([key_weight, content_projection_matrix])
-    weight = jnp.broadcast_to(weight, (chips, *weight.shape)).reshape(2 * chips, depth, columns)
+    weight = spread(key_weight, content_projection_matrix, chips)
     weight = lax.all_to_all(weight, ("x", "core"), 0, 0, tiled=True).reshape(2 * chips * depth, columns)
     rows = stage(mixer_input.reshape(seqs * block, width))
     their_rows = lax.ppermute(rows, "core", other)

time: 89.6 us -> 91.7 us (1.023)
  Pallas kernels: 8.07 us -> 11.2 us
  local copies, waits for them, and re-layouts: 2.94 us -> 1.9 us
    pallas_call x0 -> x1, Pallas kernels: none -> 1.95 us  [spread(): pl.pallas_call(spread_kernel, out_shape=jax.ShapeDtypeStruct((2 * chips,...]
    pallas_call x1, Pallas kernels: 5.01 us -> 6.18 us  [project(): pl.pallas_call(project_kernel, out_shape=jax.ShapeDtypeStruct((heads, 2 *...]
    broadcast_in_dim x1 -> x0, local copies, waits for them, and re-layouts: 1.04 us -> none  [local(): jnp.broadcast_to(weight, (chips, *weight.shape))]
    unnamed x10 -> x6, local copies, waits for them, and re-layouts: 1.9 us -> 1.9 us
  transfers between devices with their start and end apart: 3 -> 3, of which waited for: 2 -> 2; matrix products, arithmetic and copies ran while one was open for 1% -> 0% of each run, Pallas kernels for 0% -> 2%
where the time goes in v5:
time: 91.7 us; the launch traced here: 91.3 us
  blocking collectives  40.8 us (44%)
  starting transfers between devices  19.8 us (22%)
  waiting for transfers between devices  16.8 us (18%)
  Pallas kernels  11.2 us (12%)
  local copies, waits for them, and re-layouts  1.9 us (2%)
    all_to_all x1, blocking collectives, local(): mine = lax.all_to_all(packed, ('z', 'y'), 0, 0, tiled=True)  27 us
    all_to_all x1, waiting for transfers between devices, local(): lax.all_to_all(weight, ('x', 'core'), 0, 0, tiled=True)  15 us
    all_to_all x1, blocking collectives, local(): packed = lax.all_to_all(packed, 'x', 0, 0, tiled=True)  13.8 us
    ppermute x1, starting transfers between devices, local(): their_rows = lax.ppermute(rows, 'core', other)  8.75 us
    ppermute x1, starting transfers between devices, local(): theirs = lax.ppermute(mine, 'core', other)  6.85 us
    pallas_call x1, Pallas kernels, project(): pl.pallas_call(project_kernel, out_shape=jax.ShapeDtypeStruct((heads, 2 *...  6.18 us
    all_to_all x1, starting transfers between devices, local(): lax.all_to_all(weight, ('x', 'core'), 0, 0, tiled=True)  4.22 us
    pallas_call x1, Pallas kernels, read(): pl.pallas_call(read_kernel, out_shape=(jax.ShapeDtypeStruct((1, 1, span,...  2.85 us
  transfers between devices with their start and end apart: 3, of which 2 were waited for; matrix products, arithmetic and copies ran while one was open for 0% of the time, Pallas kernels for 2%

profile of v5, /device:TPU:1, one launch (start us, length us, event | category | flops | bytes accessed | tf_op | source)
XLA Modules:
  0.0 91.3 jit_solution(8712432234163666960)
XLA Ops:
  0.6 0.0 copy-start
  0.6 1.9 %copy-done = bf16[4,192,2048]{2,1,0:T(8,128)(2,1)S(1)} copy-done((bf16[4,192,2048]{2,1,0:T(8,128)(2,1)S(1)}, bf16[4,192,2048]{2,1,0:T(8,128)(2,1)}, u32[]{:S(2)}) %copy-start) | copy-done | bytes 3145752
  2.5 0.2 shard_map.68.mine_ref
  2.7 8.7 %collective-permute-start = (bf16[768,2048]{1,0:T(8,128)(2,1)S(1)}, bf16[768,2048]{1,0:T(8,128)(2,1)}, u32[]{:S(2)}, u32[]{:S(2)}) collective-permute-start(bf16[768,2048]{1,0:T(8,128)(2,1)S(1)} %shard_map.68.mine_ref), channel_id=1, source_target_pairs={{0,1},{1,0},{2,3},{3,2},{4,5},{5,4},{6,7},{7,6},{8,9},{9,8},{10,11... | collective-permute-start | bytes 9437192 | tf_op jit(solution)/shard_map/ppermute | solution.py:197
  11.5 1.9 %shard_map.69 = bf16[8,256,256]{2,1,0:T(8,128)(2,1)} custom-call(bf16[256,256]{1,0:T(8,128)(2,1)} %key_ref.1, bf16[256,256]{1,0:T(8,128)(2,1)} %value_ref.1), custom_call_target="tpu_custom_call" | custom-call | flops 1048576 | bytes 2097152 | tf_op jit(solution)/shard_map/pallas_call | solution.py:51
  13.5 4.2 %all-to-all-start = ((bf16[8,256,256]{2,1,0:T(8,128)(2,1)}), bf16[8,256,256]{2,1,0:T(8,128)(2,1)}, u32[]{:S(2)}, u32[]{:S(2)}) async-start(bf16[8,256,256]{2,1,0:T(8,128)(2,1)} %shard_map.69), calls=%async_computation | async-start | bytes 2097152 | tf_op jit(solution)/shard_map/all_to_all | solution.py:195
  17.7 15.0 %all-to-all-done = bf16[8,256,256]{2,1,0:T(8,128)(2,1)} async-done(((bf16[8,256,256]{2,1,0:T(8,128)(2,1)}), bf16[8,256,256]{2,1,0:T(8,128)(2,1)}, u32[]{:S(2)}, u32[]{:S(2)}) %all-to-all-start) | async-done | bytes 1048608 | tf_op jit(solution)/shard_map/all_to_all | solution.py:195
  32.7 0.0 collective-permute-done.other_hbm
  32.7 6.2 %shard_map.70 = bf16[4,8,96,128]{3,2,1,0:T(8,128)(2,1)S(1)} custom-call(s32[1]{0:T(128)} %bitcast.core_ref, bf16[768,2048]{1,0:T(8,128)(2,1)S(1)} %shard_map.68.mine_ref, bf16[768,2048]{1,0:T(8,128)(2,1)} %collective-permute-done.other_hbm, bf16[2048,256]{1,0:T(8,128)(2,1)} %bitcast.3.w_hbm), custom_call_target="tpu_custom_call" | custom-call | flops 1610612736 | bytes 8388608 | tf_op jit(solution)/shard_map/pallas_call | solution.py:97
  38.9 0.0 copy-start.1
  38.9 0.0 copy-start.2
  38.9 13.8 %all_to_all.15 = bf16[4,8,96,128]{3,2,1,0:T(8,128)(2,1)S(1)} all-to-all(bf16[4,8,96,128]{3,2,1,0:T(8,128)(2,1)S(1)} %shard_map.70), channel_id=1, replica_groups=mesh['gr'=2,'z'=4,'y'=8,'x'=4,'core'=2] {'x'}, dimensions={0} | all-to-all | bytes 1572864 | tf_op jit(solution)/shard_map/all_to_all | solution.py:199
  52.8 27.0 %all_to_all.16.mine_ref = bf16[32,96,128]{2,1,0:T(8,128)(2,1)S(1)} all-to-all(bf16[32,96,128]{2,1,0:T(8,128)(2,1)S(1)} %bitcast.6), channel_id=1, replica_groups=mesh['gr'=2,'z'=4,'y'=8,'x'=4,'core'=2] {'z','y'}, dimensions={0} | all-to-all | bytes 1572864 | tf_op jit(solution)/shard_map/all_to_all | solution.py:201
  79.7 6.9 %collective-permute-start.1 = (bf16[32,96,128]{2,1,0:T(8,128)(2,1)S(1)}, bf16[32,96,128]{2,1,0:T(8,128)(2,1)S(1)}, u32[]{:S(2)}, u32[]{:S(2)}) collective-permute-start(bf16[32,96,128]{2,1,0:T(8,128)(2,1)S(1)} %all_to_all.16.mine_ref), channel_id=1, source_target_pairs={{0,1},{1,0},{2,3},{3,2},{4,5},{5,4},{6,7},{7,6},{8,9},{9,8},{10,11... | collective-permute-start | bytes 2359304 | tf_op jit(solution)/shard_map/ppermute | solution.py:202
  86.6 0.1 pad_add_fusion.info_ref
  86.7 1.8 %collective-permute-done.1.other_ref = bf16[32,96,128]{2,1,0:T(8,128)(2,1)S(1)} collective-permute-done((bf16[32,96,128]{2,1,0:T(8,128)(2,1)S(1)}, bf16[32,96,128]{2,1,0:T(8,128)(2,1)S(1)}, u32[]{:S(2)}, u32[]{:S(2)}) %collective-permute-start.1) | collective-permute-done | bytes 786464 | tf_op jit(solution)/shard_map/ppermute | solution.py:202
  88.5 0.0 copy-done.1
  88.5 0.0 copy-done.2
  88.5 2.8 %shard_map.71 = (bf16[1,1,6144,128]{3,2,1,0:T(8,128)(2,1)}, bf16[1,4,64]{2,1,0:T(4,128)(2,1)}) custom-call(s32[2]{0:T(128)S(1)} %pad_add_fusion.info_ref, f32[32]{0:T(128)S(1)} %copy-done.2, bf16[32,96,128]{2,1,0:T(8,128)(2,1)S(1)} %all_to_all.16.mine_ref, bf16[32,96,128]{2,1,0:T(8,128)(2,1)S(1)} %collective-permute-done.1.other_ref, ...), custom_call_target="tpu_custom_call" | custom-call | flops 25165824 | bytes 4194304 | tf_op jit(solution)/shard_map/pallas_call | solution.py:176
Async XLA Ops:
  0.6 1.9 %copy-start = (bf16[4,192,2048]{2,1,0:T(8,128)(2,1)S(1)}, bf16[4,192,2048]{2,1,0:T(8,128)(2,1)}, u32[]{:S(2)}) copy-start(bf16[4,192,2048]{2,1,0:T(8,128)(2,1)} %param.5) | copy-start | bytes 9437188
  2.7 30.0 %collective-permute-start = (bf16[768,2048]{1,0:T(8,128)(2,1)S(1)}, bf16[768,2048]{1,0:T(8,128)(2,1)}, u32[]{:S(2)}, u32[]{:S(2)}) collective-permute-start(bf16[768,2048]{1,0:T(8,128)(2,1)S(1)} %shard_map.68.mine_ref), channel_id=1, source_target_pairs={{0,1},{1,0},{2,3},{3,2},{4,5},{5,4},{6,7},{7,6},{8,9},{9,8},{10,11... | collective-permute-start | bytes 9437192 | tf_op jit(solution)/shard_map/ppermute | solution.py:197
  13.5 19.2 %all-to-all-start = ((bf16[8,256,256]{2,1,0:T(8,128)(2,1)}), bf16[8,256,256]{2,1,0:T(8,128)(2,1)}, u32[]{:S(2)}, u32[]{:S(2)}) async-start(bf16[8,256,256]{2,1,0:T(8,128)(2,1)} %shard_map.69), calls=%async_computation | async-start | bytes 2097152 | tf_op jit(solution)/shard_map/all_to_all | solution.py:195
  38.9 49.6 %copy-start.1 = (bf16[1,4,64]{2,1,0:T(4,128)(2,1)S(1)}, bf16[1,4,64]{2,1,0:T(4,128)(2,1)}, u32[]{:S(2)}) copy-start(bf16[1,4,64]{2,1,0:T(4,128)(2,1)} %q_ref.1) | copy-start | bytes 1540
  38.9 49.6 %copy-start.2 = (f32[32]{0:T(128)S(1)}, f32[32]{0:T(128)}, u32[]{:S(2)}) copy-start(f32[32]{0:T(128)} %off_ref.1) | copy-start | bytes 388
  79.7 8.7 %collective-permute-start.1 = (bf16[32,96,128]{2,1,0:T(8,128)(2,1)S(1)}, bf16[32,96,128]{2,1,0:T(8,128)(2,1)S(1)}, u32[]{:S(2)}, u32[]{:S(2)}) collective-permute-start(bf16[32,96,128]{2,1,0:T(8,128)(2,1)S(1)} %all_to_all.16.mine_ref), channel_id=1, source_target_pairs={{0,1},{1,0},{2,3},{3,2},{4,5},{5,4},{6,7},{7,6},{8,9},{9,8},{10,11... | collective-permute-start | bytes 2359304 | tf_op jit(solution)/shard_map/ppermute | solution.py:202

commit v6 on v2

--- a/solution.py
+++ b/solution.py
@@ -9,32 +9,32 @@
 F32, BF16 = jnp.float32, jnp.bfloat16
 SMEM = pl.BlockSpec(memory_space=pltpu.SMEM)
 VMEM = pl.BlockSpec(memory_space=pltpu.VMEM)
-ANY = pl.BlockSpec(memory_space=pl.ANY)
+HBM = pl.BlockSpec(memory_space=pltpu.HBM)
+GRANT = pltpu.CompilerParams(vmem_limit_bytes=16 << 20)
 
 
-def project_kernel(core_ref, mine_ref, other_ref, w_ref, out_ref):
-    core = core_ref[0]
+def project_kernel(mine_ref, other_ref, w_ref, out_ref):
+    core = lax.axis_index("core")
     heads, both, half, _ = out_ref.shape
-    seq = pl.program_id(0)
+    seqs = both // 2
     for ref, which in ((mine_ref, core), (other_ref, 1 - core)):
         rows = jnp.dot(ref[...], w_ref[...], preferred_element_type=F32)
-        for h in range(heads):
-            part = rows[:, HEAD_DIM * h : HEAD_DIM * h + HEAD_DIM]
-            out_ref[h, which * (both // 2) + seq] = jnp.concatenate([part[:half], part[half:]], axis=1).astype(BF16)
+        for i in range(seqs):
+            for h in range(heads):
+                part = rows[2 * half * i : 2 * half * (i + 1), HEAD_DIM * h : HEAD_DIM * h + HEAD_DIM]
+                out_ref[h, which * seqs + i] = jnp.concatenate([part[:half], part[half:]], axis=1).astype(BF16)
 
 
-def project(core, mine, other, w, seqs, half):
+def project(mine, other, w, seqs, half):
     heads = w.shape[1] // HEAD_DIM
-    rows = pl.BlockSpec((2 * half, w.shape[0]), lambda i: (i, 0))
     return pl.pallas_call(
         project_kernel,
         out_shape=jax.ShapeDtypeStruct((heads, 2 * seqs, half, 128), BF16),
-        grid=(seqs,),
-        in_specs=[SMEM, rows, rows, pl.BlockSpec(w.shape, lambda i: (0, 0))],
-        out_specs=pl.BlockSpec((heads, 2 * seqs, half, 128), lambda i: (0, 0, 0, 0)),
-        compiler_params=pltpu.CompilerParams(vmem_limit_bytes=24 << 20),
+        in_specs=[VMEM, VMEM, VMEM],
+        out_specs=VMEM,
+        compiler_params=GRANT,
         cost_estimate=pl.CostEstimate(flops=4 * mine.shape[0] * w.shape[0] * w.shape[1], bytes_accessed=8 << 20, transcendentals=0),
-    )(core, mine, other, w)
+    )(mine, other, w)
 
 
 def split3(a):
@@ -47,11 +47,12 @@
 PARTS = 4
 
 
-def read_kernel(info_ref, off_ref, mine_ref, other_ref, q_ref, cache_ref, out_ref, kv_ref, sems):
+def read_kernel(off_ref, mine_ref, other_ref, q_ref, cache_ref, out_ref, kv_ref, sems):
     blocks, half, width = mine_ref.shape
     span = kv_ref.shape[0]
     group = q_ref.shape[1]
-    core, first = info_ref[0], info_ref[1]
+    core = lax.axis_index("core")
+    first = (lax.axis_index("x") * 2 + core) * group
     swap = core == 1
     piece = span // PARTS
     copies = []
@@ -102,40 +103,38 @@
         copy.wait()
 
 
-def read(info, off, mine, other, q):
+def read(off, mine, other, q):
     blocks, half, width = mine.shape
     span = 2 * blocks * half
     group = q.shape[1]
     return pl.pallas_call(
         read_kernel,
         out_shape=(jax.ShapeDtypeStruct((1, 1, span, width), BF16), jax.ShapeDtypeStruct(q.shape, BF16)),
-        in_specs=[SMEM, SMEM, VMEM, VMEM, VMEM],
-        out_specs=(ANY, VMEM),
+        in_specs=[SMEM, VMEM, VMEM, VMEM],
+        out_specs=(HBM, VMEM),
         scratch_shapes=[pltpu.VMEM((span, width), BF16), pltpu.SemaphoreType.DMA((PARTS,))],
-        compiler_params=pltpu.CompilerParams(vmem_limit_bytes=24 << 20),
+        compiler_params=GRANT,
         cost_estimate=pl.CostEstimate(flops=32 * span * width, bytes_accessed=4 << 20, transcendentals=24 * span),
-    )(info, off, mine, other, q)
+    )(off, mine, other, q)
 
 
 def local(mixer_input, key_weight, content_projection_matrix, new_queries, head_stick_offset):
     seqs, block, width = mixer_input.shape
     depth, columns = key_weight.shape
     half = block // 2
-    core = lax.axis_index("core").astype(jnp.int32)
     other = [(0, 1), (1, 0)]
+    chips = lax.axis_size("x")
     rows = mixer_input.reshape(seqs * block, width)
     their_rows = lax.ppermute(rows, "core", other)
-    chips = lax.axis_size("x")
     weight = jnp.stack([key_weight, content_projection_matrix])
     weight = jnp.broadcast_to(weight, (chips, *weight.shape)).reshape(2 * chips, depth, columns)
     weight = lax.all_to_all(weight, ("x", "core"), 0, 0, tiled=True).reshape(2 * chips * depth, columns)
-    packed = project(core.reshape(1), rows, their_rows, weight, seqs, half)
+    packed = project(rows, their_rows, weight, seqs, half)
     packed = lax.all_to_all(packed, "x", 0, 0, tiled=True)
     packed = packed.reshape(packed.shape[0] * 2 * seqs, half, 128)
     mine = lax.all_to_all(packed, ("z", "y"), 0, 0, tiled=True)
     theirs = lax.ppermute(mine, "core", other)
-    first = (lax.axis_index("x") * 2 + core) * new_queries.shape[1]
-    return read(jnp.stack([core, first]), head_stick_offset, mine, theirs, new_queries)
+    return read(head_stick_offset, mine, theirs, new_queries)
 
 
 def solution(mesh):

time: 89.6 us -> 84.1 us (0.939)
  blocking collectives: 41.5 us -> 59.5 us
  waiting for transfers between devices: 16.8 us -> 1.89 us
  starting transfers between devices: 19.1 us -> 15.9 us
  local copies, waits for them, and re-layouts: 2.94 us -> 0.09 us
  Pallas kernels: 7.14 us -> 4.71 us
    all_to_all x0 -> x1, blocking collectives: none -> 17.4 us  [local(): lax.all_to_all(weight, ('x', 'core'), 0, 0, tiled=True)]
    all_to_all x1 -> x0, waiting for transfers between devices: 14.9 us -> none  [local(): lax.all_to_all(weight, ('x', 'core'), 0, 0, tiled=True)]
    all_to_all x1 -> x0, starting transfers between devices: 3.51 us -> none  [local(): lax.all_to_all(weight, ('x', 'core'), 0, 0, tiled=True)]
    pallas_call x1, Pallas kernels: 4.33 us -> 1.86 us  [project(): pl.pallas_call(project_kernel, out_shape=jax.ShapeDtypeStruct((heads, 2 *...]
    unnamed x6, local copies, waits for them, and re-layouts: 1.9 us -> 0.02 us
    broadcast_in_dim x1, local copies, waits for them, and re-layouts: 1.04 us -> 0.07 us  [local(): jnp.broadcast_to(weight, (chips, *weight.shape))]
  transfers between devices with their start and end apart: 3 -> 2, of which waited for: 2 -> 1; matrix products, arithmetic and copies ran while one was open for 2% -> 1% of each run, Pallas kernels for 0% -> 0%
where the time goes in v6:
time: 84.1 us; the launch traced here: 83.8 us
  blocking collectives  59.5 us (71%)
  starting transfers between devices  15.9 us (19%)
  Pallas kernels  4.71 us (6%)
  waiting for transfers between devices  1.89 us (2%)
  other arithmetic  0.99 us (1%)
    all_to_all x1, blocking collectives, local(): mine = lax.all_to_all(packed, ('z', 'y'), 0, 0, tiled=True)  28.4 us
    all_to_all x1, blocking collectives, local(): lax.all_to_all(weight, ('x', 'core'), 0, 0, tiled=True)  17.4 us
    all_to_all x1, blocking collectives, local(): packed = lax.all_to_all(packed, 'x', 0, 0, tiled=True)  13.7 us
    ppermute x1, starting transfers between devices, local(): their_rows = lax.ppermute(rows, 'core', other)  9.01 us
    ppermute x1, starting transfers between devices, local(): theirs = lax.ppermute(mine, 'core', other)  6.93 us
    pallas_call x1, Pallas kernels, read(): pl.pallas_call(read_kernel, out_shape=(jax.ShapeDtypeStruct((1, 1, span,...  2.85 us
    ppermute x1, waiting for transfers between devices, local(): theirs = lax.ppermute(mine, 'core', other)  1.89 us
    pallas_call x1, Pallas kernels, project(): pl.pallas_call(project_kernel, out_shape=jax.ShapeDtypeStruct((heads, 2 *...  1.86 us
  transfers between devices with their start and end apart: 2, of which 1 were waited for; matrix products, arithmetic and copies ran while one was open for 1% of the time, Pallas kernels for 0%

profile of v6, /device:TPU:1, one launch (start us, length us, event | category | flops | bytes accessed | tf_op | source)
XLA Modules:
  0.0 83.8 jit_solution(12901532539210600487)
XLA Ops:
  0.6 0.0 copy-start
  0.6 9.0 %collective-permute-start = (bf16[768,2048]{1,0:T(8,128)(2,1)}, bf16[768,2048]{1,0:T(8,128)(2,1)S(1)}, u32[]{:S(2)}, u32[]{:S(2)}) collective-permute-start(bf16[768,2048]{1,0:T(8,128)(2,1)} %bitcast.7), channel_id=1, source_target_pairs={{0,1},{1,0},{2,3},{3,2},{4,5},{5,4},{6,7},{7,6},{8,9},{9,8},{10,11... | collective-permute-start | bytes 9437192 | tf_op jit(solution)/shard_map/ppermute | solution.py:128
  9.7 1.0 %pad_maximum_fusion = bf16[2,256,256]{2,1,0:T(8,128)(2,1)S(1)} fusion(bf16[1,256,256]{2,1,0:T(8,128)(2,1)} %bitcast.11, bf16[1,256,256]{2,1,0:T(8,128)(2,1)} %bitcast.12), kind=kLoop, calls=%fused_computation | loop fusion | flops 131072 | bytes 524288 | tf_op jit(solution)/shard_map/stack | solution.py:129
  10.7 0.1 broadcast_in_dim.3
  10.7 17.4 %all_to_all.15 = bf16[8,256,256]{2,1,0:T(8,128)(2,1)S(1)} all-to-all(bf16[8,256,256]{2,1,0:T(8,128)(2,1)S(1)} %bitcast.9), channel_id=1, replica_groups=mesh['gr'=2,'z'=4,'y'=8,'x'=4,'core'=2] {'x','core'}, dimensions={0} | all-to-all | bytes 2097152 | tf_op jit(solution)/shard_map/all_to_all | solution.py:131
  28.1 0.0 collective-permute-done.other_ref
  28.1 0.0 copy-done
  28.1 1.9 %shard_map.68 = bf16[4,8,96,128]{3,2,1,0:T(8,128)(2,1)S(1)} custom-call(bf16[768,2048]{1,0:T(8,128)(2,1)S(1)} %bitcast.8, bf16[768,2048]{1,0:T(8,128)(2,1)S(1)} %collective-permute-done.other_ref, bf16[2048,256]{1,0:T(8,128)(2,1)S(1)} %bitcast.6), custom_call_target="tpu_custom_call" | custom-call | flops 1610612736 | bytes 8388608 | tf_op jit(solution)/shard_map/pallas_call | solution.py:30
  30.0 0.0 copy-start.1
  30.0 0.0 copy-start.2
  30.0 13.7 %all_to_all.16 = bf16[4,8,96,128]{3,2,1,0:T(8,128)(2,1)S(1)} all-to-all(bf16[4,8,96,128]{3,2,1,0:T(8,128)(2,1)S(1)} %shard_map.68), channel_id=1, replica_groups=mesh['gr'=2,'z'=4,'y'=8,'x'=4,'core'=2] {'x'}, dimensions={0} | all-to-all | bytes 1572864 | tf_op jit(solution)/shard_map/all_to_all | solution.py:133
  43.7 28.4 %all_to_all.17.mine_ref = bf16[32,96,128]{2,1,0:T(8,128)(2,1)S(1)} all-to-all(bf16[32,96,128]{2,1,0:T(8,128)(2,1)S(1)} %bitcast.10), channel_id=1, replica_groups=mesh['gr'=2,'z'=4,'y'=8,'x'=4,'core'=2] {'z','y'}, dimensions={0} | all-to-all | bytes 1572864 | tf_op jit(solution)/shard_map/all_to_all | solution.py:135
  72.2 6.9 %collective-permute-start.1 = (bf16[32,96,128]{2,1,0:T(8,128)(2,1)S(1)}, bf16[32,96,128]{2,1,0:T(8,128)(2,1)S(1)}, u32[]{:S(2)}, u32[]{:S(2)}) collective-permute-start(bf16[32,96,128]{2,1,0:T(8,128)(2,1)S(1)} %all_to_all.17.mine_ref), channel_id=1, source_target_pairs={{0,1},{1,0},{2,3},{3,2},{4,5},{5,4},{6,7},{7,6},{8,9},{9,8},{10,11... | collective-permute-start | bytes 2359304 | tf_op jit(solution)/shard_map/ppermute | solution.py:136
  79.1 1.9 %collective-permute-done.1.other_ref = bf16[32,96,128]{2,1,0:T(8,128)(2,1)S(1)} collective-permute-done((bf16[32,96,128]{2,1,0:T(8,128)(2,1)S(1)}, bf16[32,96,128]{2,1,0:T(8,128)(2,1)S(1)}, u32[]{:S(2)}, u32[]{:S(2)}) %collective-permute-start.1) | collective-permute-done | bytes 786464 | tf_op jit(solution)/shard_map/ppermute | solution.py:136
  81.0 0.0 copy-done.1
  81.0 0.0 copy-done.2
  81.0 2.8 %shard_map.69 = (bf16[1,1,6144,128]{3,2,1,0:T(8,128)(2,1)}, bf16[1,4,64]{2,1,0:T(4,128)(2,1)}) custom-call(f32[32]{0:T(128)S(1)} %copy-done.2, bf16[32,96,128]{2,1,0:T(8,128)(2,1)S(1)} %all_to_all.17.mine_ref, bf16[32,96,128]{2,1,0:T(8,128)(2,1)S(1)} %collective-permute-done.1.other_ref, bf16[1,4,64]{2,1,0:T(4,128)(2,1)S(1)} %copy-done.1), custom_call_target="tpu_custom_call" | custom-call | flops 25165824 | bytes 4194304 | tf_op jit(solution)/shard_map/pallas_call | solution.py:110
Async XLA Ops:
  0.6 27.5 %copy-start = (bf16[4,192,2048]{2,1,0:T(8,128)(2,1)S(1)}, bf16[4,192,2048]{2,1,0:T(8,128)(2,1)}, u32[]{:S(2)}) copy-start(bf16[4,192,2048]{2,1,0:T(8,128)(2,1)} %param.5) | copy-start | bytes 9437188
  0.6 27.5 %collective-permute-start = (bf16[768,2048]{1,0:T(8,128)(2,1)}, bf16[768,2048]{1,0:T(8,128)(2,1)S(1)}, u32[]{:S(2)}, u32[]{:S(2)}) collective-permute-start(bf16[768,2048]{1,0:T(8,128)(2,1)} %bitcast.7), channel_id=1, source_target_pairs={{0,1},{1,0},{2,3},{3,2},{4,5},{5,4},{6,7},{7,6},{8,9},{9,8},{10,11... | collective-permute-start | bytes 9437192 | tf_op jit(solution)/shard_map/ppermute | solution.py:128
  30.0 51.0 %copy-start.1 = (bf16[1,4,64]{2,1,0:T(4,128)(2,1)S(1)}, bf16[1,4,64]{2,1,0:T(4,128)(2,1)}, u32[]{:S(2)}) copy-start(bf16[1,4,64]{2,1,0:T(4,128)(2,1)} %q_ref.1) | copy-start | bytes 1540
  30.0 51.0 %copy-start.2 = (f32[32]{0:T(128)S(1)}, f32[32]{0:T(128)}, u32[]{:S(2)}) copy-start(f32[32]{0:T(128)} %off_ref.1) | copy-start | bytes 388
  72.2 8.8 %collective-permute-start.1 = (bf16[32,96,128]{2,1,0:T(8,128)(2,1)S(1)}, bf16[32,96,128]{2,1,0:T(8,128)(2,1)S(1)}, u32[]{:S(2)}, u32[]{:S(2)}) collective-permute-start(bf16[32,96,128]{2,1,0:T(8,128)(2,1)S(1)} %all_to_all.17.mine_ref), channel_id=1, source_target_pairs={{0,1},{1,0},{2,3},{3,2},{4,5},{5,4},{6,7},{7,6},{8,9},{9,8},{10,11... | collective-permute-start | bytes 2359304 | tf_op jit(solution)/shard_map/ppermute | solution.py:136

commit v7 on v6

--- a/solution.py
+++ b/solution.py
@@ -1,5 +1,6 @@
 import jax
 import jax.numpy as jnp
+import numpy as np
 from jax import lax
 from jax.experimental import pallas as pl
 from jax.experimental.pallas import tpu as pltpu
@@ -17,23 +18,27 @@
     core = lax.axis_index("core")
     heads, both, half, _ = out_ref.shape
     seqs = both // 2
+    depth = w_ref.shape[1]
     for ref, which in ((mine_ref, core), (other_ref, 1 - core)):
-        rows = jnp.dot(ref[...], w_ref[...], preferred_element_type=F32)
+        rows = None
+        for n, shard in enumerate(SHARD_OF):
+            part = jnp.dot(ref[:, depth * shard : depth * (shard + 1)], w_ref[n], preferred_element_type=F32)
+            rows = part if rows is None else rows + part
         for i in range(seqs):
             for h in range(heads):
                 part = rows[2 * half * i : 2 * half * (i + 1), HEAD_DIM * h : HEAD_DIM * h + HEAD_DIM]
-                out_ref[h, which * seqs + i] = jnp.concatenate([part[:half], part[half:]], axis=1).astype(BF16)
+                out_ref[CHIP_AT[h], which * seqs + i] = jnp.concatenate([part[:half], part[half:]], axis=1).astype(BF16)
 
 
 def project(mine, other, w, seqs, half):
-    heads = w.shape[1] // HEAD_DIM
+    heads = w.shape[2] // HEAD_DIM
     return pl.pallas_call(
         project_kernel,
         out_shape=jax.ShapeDtypeStruct((heads, 2 * seqs, half, 128), BF16),
         in_specs=[VMEM, VMEM, VMEM],
         out_specs=VMEM,
         compiler_params=GRANT,
-        cost_estimate=pl.CostEstimate(flops=4 * mine.shape[0] * w.shape[0] * w.shape[1], bytes_accessed=8 << 20, transcendentals=0),
+        cost_estimate=pl.CostEstimate(flops=4 * mine.shape[0] * mine.shape[1] * w.shape[2], bytes_accessed=8 << 20, transcendentals=0),
     )(mine, other, w)
 
 
@@ -45,6 +50,20 @@
 
 
 PARTS = 4
+BITS = ("z1", "z0", "y2", "y1", "y0")
+LINE = ("x1", "x0")
+WEIGHT_ORDER = ("x0", "core", "x1")
+CHIP_ORDER = ("x0", "x1")
+ORDER = ("y2", "z1", "y1", "z0", "y0")
+
+
+def places(names, order):
+    return np.arange(2 ** len(names)).reshape([2] * len(names)).transpose([order.index(n) for n in names]).ravel().tolist()
+
+
+SHARD_OF = places(WEIGHT_ORDER, (*LINE, "core"))
+CHIP_AT = places(LINE, CHIP_ORDER)
+BLOCK_AT = places(BITS, ORDER)
 
 
 def read_kernel(off_ref, mine_ref, other_ref, q_ref, cache_ref, out_ref, kv_ref, sems):
@@ -52,12 +71,12 @@
     span = kv_ref.shape[0]
     group = q_ref.shape[1]
     core = lax.axis_index("core")
-    first = (lax.axis_index("x") * 2 + core) * group
+    first = ((lax.axis_index("x1") * 2 + lax.axis_index("x0")) * 2 + core) * group
     swap = core == 1
     piece = span // PARTS
     copies = []
-    for b in range(blocks):
-        a, o = mine_ref[b], other_ref[b]
+    for b, n in enumerate(BLOCK_AT):
+        a, o = mine_ref[n], other_ref[n]
         keys = jnp.where(swap, o, a)
         values = jnp.where(swap, a, o)
         base = 2 * half * b
@@ -123,23 +142,24 @@
     depth, columns = key_weight.shape
     half = block // 2
     other = [(0, 1), (1, 0)]
-    chips = lax.axis_size("x")
     rows = mixer_input.reshape(seqs * block, width)
     their_rows = lax.ppermute(rows, "core", other)
-    weight = jnp.stack([key_weight, content_projection_matrix])
-    weight = jnp.broadcast_to(weight, (chips, *weight.shape)).reshape(2 * chips, depth, columns)
-    weight = lax.all_to_all(weight, ("x", "core"), 0, 0, tiled=True).reshape(2 * chips * depth, columns)
+    pair = jnp.stack([key_weight, content_projection_matrix])
+    shape = [2 if name == "core" else 1 for name in WEIGHT_ORDER]
+    weight = jnp.broadcast_to(pair.reshape(*shape, depth, columns), (2, 2, 2, depth, columns)).reshape(8, depth, columns)
+    weight = lax.all_to_all(weight, WEIGHT_ORDER, 0, 0, tiled=True)
     packed = project(rows, their_rows, weight, seqs, half)
-    packed = lax.all_to_all(packed, "x", 0, 0, tiled=True)
-    packed = packed.reshape(packed.shape[0] * 2 * seqs, half, 128)
-    mine = lax.all_to_all(packed, ("z", "y"), 0, 0, tiled=True)
+    packed = lax.all_to_all(packed, CHIP_ORDER, 0, 0, tiled=True)
+    held = (*(name.replace("x", "z") for name in CHIP_ORDER), "y2", "y1", "y0")
+    packed = packed.reshape(2, 2, 2, 2, 2, half, 128).transpose(*(held.index(n) for n in ORDER), 5, 6).reshape(-1, half, 128)
+    mine = lax.all_to_all(packed, ORDER, 0, 0, tiled=True)
     theirs = lax.ppermute(mine, "core", other)
     return read(head_stick_offset, mine, theirs, new_queries)
 
 
 def solution(mesh):
-    wide = Mesh(mesh.devices.reshape(2, 4, 8, 4, 2), ("gr", "z", "y", "x", "core"))
-    sp, tp = ("z", "y"), ("x", "core")
+    wide = Mesh(mesh.devices.reshape([2] * 9), ("gr", *BITS, *LINE, "core"))
+    sp, tp = BITS, (*LINE, "core")
     return jax.shard_map(
         local,
         mesh=wide,

time: 84.1 us -> 83.2 us (0.989)
  starting transfers between devices: 15.9 us -> 14.5 us
    ppermute x1, starting transfers between devices: 6.93 us -> 5.49 us  [local(): theirs = lax.ppermute(mine, 'core', other)]
where the time goes in v7:
time: 83.2 us; the launch traced here: 82.9 us
  blocking collectives  60 us (72%)
  starting transfers between devices  14.5 us (17%)
  Pallas kernels  4.71 us (6%)
  waiting for transfers between devices  1.89 us (2%)
  other arithmetic  0.99 us (1%)
    all_to_all x1, blocking collectives, local(): mine = lax.all_to_all(packed, ORDER, 0, 0, tiled=True)  29 us
    all_to_all x1, blocking collectives, local(): weight = lax.all_to_all(weight, WEIGHT_ORDER, 0, 0, tiled=True)  17.4 us
    all_to_all x1, blocking collectives, local(): packed = lax.all_to_all(packed, CHIP_ORDER, 0, 0, tiled=True)  13.6 us
    ppermute x1, starting transfers between devices, local(): their_rows = lax.ppermute(rows, 'core', other)  9.01 us
    ppermute x1, starting transfers between devices, local(): theirs = lax.ppermute(mine, 'core', other)  5.49 us
    pallas_call x1, Pallas kernels, read(): pl.pallas_call(read_kernel, out_shape=(jax.ShapeDtypeStruct((1, 1, span,...  2.84 us
    ppermute x1, waiting for transfers between devices, local(): theirs = lax.ppermute(mine, 'core', other)  1.89 us
    pallas_call x1, Pallas kernels, project(): pl.pallas_call(project_kernel, out_shape=jax.ShapeDtypeStruct((heads, 2 *...  1.86 us
  transfers between devices with their start and end apart: 2, of which 1 were waited for; matrix products, arithmetic and copies ran while one was open for 1% of the time, Pallas kernels for 0%

profile of v7, /device:TPU:1, one launch (start us, length us, event | category | flops | bytes accessed | tf_op | source)
XLA Modules:
  0.0 82.9 jit_solution(4640944272678040529)
XLA Ops:
  0.6 0.0 copy-start
  0.6 9.0 %collective-permute-start = (bf16[768,2048]{1,0:T(8,128)(2,1)}, bf16[768,2048]{1,0:T(8,128)(2,1)S(1)}, u32[]{:S(2)}, u32[]{:S(2)}) collective-permute-start(bf16[768,2048]{1,0:T(8,128)(2,1)} %bitcast.8), channel_id=1, source_target_pairs={{0,1},{1,0},{2,3},{3,2},{4,5},{5,4},{6,7},{7,6},{8,9},{9,8},{10,11... | collective-permute-start | bytes 9437192 | tf_op jit(solution)/shard_map/ppermute | solution.py:146
  9.7 1.0 %pad_maximum_fusion = bf16[2,256,256]{2,1,0:T(8,128)(2,1)S(1)} fusion(bf16[1,256,256]{2,1,0:T(8,128)(2,1)} %bitcast.13, bf16[1,256,256]{2,1,0:T(8,128)(2,1)} %bitcast.14), kind=kLoop, calls=%fused_computation | loop fusion | flops 131072 | bytes 524288 | tf_op jit(solution)/shard_map/stack | solution.py:147
  10.7 0.1 broadcast_in_dim.2
  10.7 17.4 %all_to_all.15.w_ref = bf16[8,256,256]{2,1,0:T(8,128)(2,1)S(1)} all-to-all(bf16[8,256,256]{2,1,0:T(8,128)(2,1)S(1)} %bitcast.10), channel_id=1, replica_groups=mesh['gr'=2,'z1'=2,'z0'=2,'y2'=2,'y1'=2,'y0'=2,'x1'=2,'x0'=2,'core'=2] {..., dimensions={0} | all-to-all | bytes 2097152 | tf_op jit(solution)/shard_map/all_to_all | solution.py:150
  28.1 0.0 collective-permute-done.other_ref
  28.1 0.0 copy-done
  28.1 1.9 %shard_map.68 = bf16[4,8,96,128]{3,2,1,0:T(8,128)(2,1)S(1)} custom-call(bf16[768,2048]{1,0:T(8,128)(2,1)S(1)} %bitcast.9, bf16[768,2048]{1,0:T(8,128)(2,1)S(1)} %collective-permute-done.other_ref, bf16[8,256,256]{2,1,0:T(8,128)(2,1)S(1)} %all_to_all.15.w_ref), custom_call_target="tpu_custom_call" | custom-call | flops 1610612736 | bytes 8388608 | tf_op jit(solution)/shard_map/pallas_call | solution.py:35
  30.0 0.0 copy-start.1
  30.0 0.0 copy-start.2
  30.0 13.6 %all_to_all.16 = bf16[4,8,96,128]{3,2,1,0:T(8,128)(2,1)S(1)} all-to-all(bf16[4,8,96,128]{3,2,1,0:T(8,128)(2,1)S(1)} %shard_map.68), channel_id=1, replica_groups=mesh['gr'=2,'z1'=2,'z0'=2,'y2'=2,'y1'=2,'y0'=2,'x1'=2,'x0'=2,'core'=2] {..., dimensions={0} | all-to-all | bytes 1572864 | tf_op jit(solution)/shard_map/all_to_all | solution.py:152
  43.6 0.1 copy.7
  43.7 29.0 %all_to_all.17.mine_ref = bf16[32,96,128]{2,1,0:T(8,128)(2,1)S(1)} all-to-all(bf16[32,96,128]{2,1,0:T(8,128)(2,1)S(1)} %bitcast.12), channel_id=1, replica_groups=mesh['gr'=2,'z1'=2,'z0'=2,'y2'=2,'y1'=2,'y0'=2,'x1'=2,'x0'=2,'core'=2] {..., dimensions={0} | all-to-all | bytes 1572864 | tf_op jit(solution)/shard_map/all_to_all | solution.py:155
  72.7 5.5 %collective-permute-start.1 = (bf16[32,96,128]{2,1,0:T(8,128)(2,1)S(1)}, bf16[32,96,128]{2,1,0:T(8,128)(2,1)S(1)}, u32[]{:S(2)}, u32[]{:S(2)}) collective-permute-start(bf16[32,96,128]{2,1,0:T(8,128)(2,1)S(1)} %all_to_all.17.mine_ref), channel_id=1, source_target_pairs={{0,1},{1,0},{2,3},{3,2},{4,5},{5,4},{6,7},{7,6},{8,9},{9,8},{10,11... | collective-permute-start | bytes 2359304 | tf_op jit(solution)/shard_map/ppermute | solution.py:156
  78.2 1.9 %collective-permute-done.1.other_ref = bf16[32,96,128]{2,1,0:T(8,128)(2,1)S(1)} collective-permute-done((bf16[32,96,128]{2,1,0:T(8,128)(2,1)S(1)}, bf16[32,96,128]{2,1,0:T(8,128)(2,1)S(1)}, u32[]{:S(2)}, u32[]{:S(2)}) %collective-permute-start.1) | collective-permute-done | bytes 786464 | tf_op jit(solution)/shard_map/ppermute | solution.py:156
  80.1 0.0 copy-done.1
  80.1 0.0 copy-done.2
  80.1 2.8 %shard_map.69 = (bf16[1,1,6144,128]{3,2,1,0:T(8,128)(2,1)}, bf16[1,4,64]{2,1,0:T(4,128)(2,1)}) custom-call(f32[32]{0:T(128)S(1)} %copy-done.2, bf16[32,96,128]{2,1,0:T(8,128)(2,1)S(1)} %all_to_all.17.mine_ref, bf16[32,96,128]{2,1,0:T(8,128)(2,1)S(1)} %collective-permute-done.1.other_ref, bf16[1,4,64]{2,1,0:T(4,128)(2,1)S(1)} %copy-done.1), custom_call_target="tpu_custom_call" | custom-call | flops 25165824 | bytes 4194304 | tf_op jit(solution)/shard_map/pallas_call | solution.py:129
Async XLA Ops:
  0.6 27.5 %copy-start = (bf16[4,192,2048]{2,1,0:T(8,128)(2,1)S(1)}, bf16[4,192,2048]{2,1,0:T(8,128)(2,1)}, u32[]{:S(2)}) copy-start(bf16[4,192,2048]{2,1,0:T(8,128)(2,1)} %param.5) | copy-start | bytes 9437188
  0.6 27.5 %collective-permute-start = (bf16[768,2048]{1,0:T(8,128)(2,1)}, bf16[768,2048]{1,0:T(8,128)(2,1)S(1)}, u32[]{:S(2)}, u32[]{:S(2)}) collective-permute-start(bf16[768,2048]{1,0:T(8,128)(2,1)} %bitcast.8), channel_id=1, source_target_pairs={{0,1},{1,0},{2,3},{3,2},{4,5},{5,4},{6,7},{7,6},{8,9},{9,8},{10,11... | collective-permute-start | bytes 9437192 | tf_op jit(solution)/shard_map/ppermute | solution.py:146
  30.0 50.1 %copy-start.1 = (bf16[1,4,64]{2,1,0:T(4,128)(2,1)S(1)}, bf16[1,4,64]{2,1,0:T(4,128)(2,1)}, u32[]{:S(2)}) copy-start(bf16[1,4,64]{2,1,0:T(4,128)(2,1)} %q_ref.1) | copy-start | bytes 1540
  30.0 50.1 %copy-start.2 = (f32[32]{0:T(128)S(1)}, f32[32]{0:T(128)}, u32[]{:S(2)}) copy-start(f32[32]{0:T(128)} %off_ref.1) | copy-start | bytes 388
  72.7 7.4 %collective-permute-start.1 = (bf16[32,96,128]{2,1,0:T(8,128)(2,1)S(1)}, bf16[32,96,128]{2,1,0:T(8,128)(2,1)S(1)}, u32[]{:S(2)}, u32[]{:S(2)}) collective-permute-start(bf16[32,96,128]{2,1,0:T(8,128)(2,1)S(1)} %all_to_all.17.mine_ref), channel_id=1, source_target_pairs={{0,1},{1,0},{2,3},{3,2},{4,5},{5,4},{6,7},{7,6},{8,9},{9,8},{10,11... | collective-permute-start | bytes 2359304 | tf_op jit(solution)/shard_map/ppermute | solution.py:156

commit v8 on v7

--- a/solution.py
+++ b/solution.py
@@ -54,7 +54,7 @@
 LINE = ("x1", "x0")
 WEIGHT_ORDER = ("x0", "core", "x1")
 CHIP_ORDER = ("x0", "x1")
-ORDER = ("y2", "z1", "y1", "z0", "y0")
+ORDER = ("y0", "y1", "z1", "z0", "y2")
 
 
 def places(names, order):

time: 83.2 us -> 82.2 us (0.988)
  blocking collectives: 60 us -> 59 us
    all_to_all x1, blocking collectives: 29 us -> 28 us  [local(): mine = lax.all_to_all(packed, ORDER, 0, 0, tiled=True)]
where the time goes in v8:
time: 82.2 us; the launch traced here: 81.7 us
  blocking collectives  59 us (72%)
  starting transfers between devices  14.2 us (17%)
  Pallas kernels  4.71 us (6%)
  waiting for transfers between devices  1.89 us (2%)
  other arithmetic  0.99 us (1%)
    all_to_all x1, blocking collectives, local(): mine = lax.all_to_all(packed, ORDER, 0, 0, tiled=True)  28 us
    all_to_all x1, blocking collectives, local(): weight = lax.all_to_all(weight, WEIGHT_ORDER, 0, 0, tiled=True)  17.4 us
    all_to_all x1, blocking collectives, local(): packed = lax.all_to_all(packed, CHIP_ORDER, 0, 0, tiled=True)  13.6 us
    ppermute x1, starting transfers between devices, local(): their_rows = lax.ppermute(rows, 'core', other)  9.01 us
    ppermute x1, starting transfers between devices, local(): theirs = lax.ppermute(mine, 'core', other)  5.19 us
    pallas_call x1, Pallas kernels, read(): pl.pallas_call(read_kernel, out_shape=(jax.ShapeDtypeStruct((1, 1, span,...  2.84 us
    ppermute x1, waiting for transfers between devices, local(): theirs = lax.ppermute(mine, 'core', other)  1.89 us
    pallas_call x1, Pallas kernels, project(): pl.pallas_call(project_kernel, out_shape=jax.ShapeDtypeStruct((heads, 2 *...  1.86 us
  transfers between devices with their start and end apart: 2, of which 1 were waited for; matrix products, arithmetic and copies ran while one was open for 1% of the time, Pallas kernels for 0%

profile of v8, /device:TPU:1, one launch (start us, length us, event | category | flops | bytes accessed | tf_op | source)
XLA Modules:
  0.0 81.7 jit_solution(18309255554025850773)
XLA Ops:
  0.6 0.0 copy-start
  0.6 9.0 %collective-permute-start = (bf16[768,2048]{1,0:T(8,128)(2,1)}, bf16[768,2048]{1,0:T(8,128)(2,1)S(1)}, u32[]{:S(2)}, u32[]{:S(2)}) collective-permute-start(bf16[768,2048]{1,0:T(8,128)(2,1)} %bitcast.8), channel_id=1, source_target_pairs={{0,1},{1,0},{2,3},{3,2},{4,5},{5,4},{6,7},{7,6},{8,9},{9,8},{10,11... | collective-permute-start | bytes 9437192 | tf_op jit(solution)/shard_map/ppermute | solution.py:146
  9.7 1.0 %pad_maximum_fusion = bf16[2,256,256]{2,1,0:T(8,128)(2,1)S(1)} fusion(bf16[1,256,256]{2,1,0:T(8,128)(2,1)} %bitcast.13, bf16[1,256,256]{2,1,0:T(8,128)(2,1)} %bitcast.14), kind=kLoop, calls=%fused_computation | loop fusion | flops 131072 | bytes 524288 | tf_op jit(solution)/shard_map/stack | solution.py:147
  10.7 0.1 broadcast_in_dim.2
  10.7 17.4 %all_to_all.15.w_ref = bf16[8,256,256]{2,1,0:T(8,128)(2,1)S(1)} all-to-all(bf16[8,256,256]{2,1,0:T(8,128)(2,1)S(1)} %bitcast.10), channel_id=1, replica_groups=mesh['gr'=2,'z1'=2,'z0'=2,'y2'=2,'y1'=2,'y0'=2,'x1'=2,'x0'=2,'core'=2] {..., dimensions={0} | all-to-all | bytes 2097152 | tf_op jit(solution)/shard_map/all_to_all | solution.py:150
  28.1 0.0 collective-permute-done.other_ref
  28.1 0.0 copy-done
  28.1 1.9 %shard_map.68 = bf16[4,8,96,128]{3,2,1,0:T(8,128)(2,1)S(1)} custom-call(bf16[768,2048]{1,0:T(8,128)(2,1)S(1)} %bitcast.9, bf16[768,2048]{1,0:T(8,128)(2,1)S(1)} %collective-permute-done.other_ref, bf16[8,256,256]{2,1,0:T(8,128)(2,1)S(1)} %all_to_all.15.w_ref), custom_call_target="tpu_custom_call" | custom-call | flops 1610612736 | bytes 8388608 | tf_op jit(solution)/shard_map/pallas_call | solution.py:35
  30.0 0.0 copy-start.1
  30.0 0.0 copy-start.2
  30.0 13.6 %all_to_all.16 = bf16[4,8,96,128]{3,2,1,0:T(8,128)(2,1)S(1)} all-to-all(bf16[4,8,96,128]{3,2,1,0:T(8,128)(2,1)S(1)} %shard_map.68), channel_id=1, replica_groups=mesh['gr'=2,'z1'=2,'z0'=2,'y2'=2,'y1'=2,'y0'=2,'x1'=2,'x0'=2,'core'=2] {..., dimensions={0} | all-to-all | bytes 1572864 | tf_op jit(solution)/shard_map/all_to_all | solution.py:152
  43.6 0.1 copy.7
  43.7 28.0 %all_to_all.17.mine_ref = bf16[32,96,128]{2,1,0:T(8,128)(2,1)S(1)} all-to-all(bf16[32,96,128]{2,1,0:T(8,128)(2,1)S(1)} %bitcast.12), channel_id=1, replica_groups=mesh['gr'=2,'z1'=2,'z0'=2,'y2'=2,'y1'=2,'y0'=2,'x1'=2,'x0'=2,'core'=2] {..., dimensions={0} | all-to-all | bytes 1572864 | tf_op jit(solution)/shard_map/all_to_all | solution.py:155
  71.8 5.2 %collective-permute-start.1 = (bf16[32,96,128]{2,1,0:T(8,128)(2,1)S(1)}, bf16[32,96,128]{2,1,0:T(8,128)(2,1)S(1)}, u32[]{:S(2)}, u32[]{:S(2)}) collective-permute-start(bf16[32,96,128]{2,1,0:T(8,128)(2,1)S(1)} %all_to_all.17.mine_ref), channel_id=1, source_target_pairs={{0,1},{1,0},{2,3},{3,2},{4,5},{5,4},{6,7},{7,6},{8,9},{9,8},{10,11... | collective-permute-start | bytes 2359304 | tf_op jit(solution)/shard_map/ppermute | solution.py:156
  77.0 1.9 %collective-permute-done.1.other_ref = bf16[32,96,128]{2,1,0:T(8,128)(2,1)S(1)} collective-permute-done((bf16[32,96,128]{2,1,0:T(8,128)(2,1)S(1)}, bf16[32,96,128]{2,1,0:T(8,128)(2,1)S(1)}, u32[]{:S(2)}, u32[]{:S(2)}) %collective-permute-start.1) | collective-permute-done | bytes 786464 | tf_op jit(solution)/shard_map/ppermute | solution.py:156
  78.9 0.0 copy-done.1
  78.9 0.0 copy-done.2
  78.9 2.8 %shard_map.69 = (bf16[1,1,6144,128]{3,2,1,0:T(8,128)(2,1)}, bf16[1,4,64]{2,1,0:T(4,128)(2,1)}) custom-call(f32[32]{0:T(128)S(1)} %copy-done.2, bf16[32,96,128]{2,1,0:T(8,128)(2,1)S(1)} %all_to_all.17.mine_ref, bf16[32,96,128]{2,1,0:T(8,128)(2,1)S(1)} %collective-permute-done.1.other_ref, bf16[1,4,64]{2,1,0:T(4,128)(2,1)S(1)} %copy-done.1), custom_call_target="tpu_custom_call" | custom-call | flops 25165824 | bytes 4194304 | tf_op jit(solution)/shard_map/pallas_call | solution.py:129
Async XLA Ops:
  0.6 27.5 %copy-start = (bf16[4,192,2048]{2,1,0:T(8,128)(2,1)S(1)}, bf16[4,192,2048]{2,1,0:T(8,128)(2,1)}, u32[]{:S(2)}) copy-start(bf16[4,192,2048]{2,1,0:T(8,128)(2,1)} %param.5) | copy-start | bytes 9437188
  0.6 27.5 %collective-permute-start = (bf16[768,2048]{1,0:T(8,128)(2,1)}, bf16[768,2048]{1,0:T(8,128)(2,1)S(1)}, u32[]{:S(2)}, u32[]{:S(2)}) collective-permute-start(bf16[768,2048]{1,0:T(8,128)(2,1)} %bitcast.8), channel_id=1, source_target_pairs={{0,1},{1,0},{2,3},{3,2},{4,5},{5,4},{6,7},{7,6},{8,9},{9,8},{10,11... | collective-permute-start | bytes 9437192 | tf_op jit(solution)/shard_map/ppermute | solution.py:146
  30.0 48.9 %copy-start.1 = (bf16[1,4,64]{2,1,0:T(4,128)(2,1)S(1)}, bf16[1,4,64]{2,1,0:T(4,128)(2,1)}, u32[]{:S(2)}) copy-start(bf16[1,4,64]{2,1,0:T(4,128)(2,1)} %q_ref.1) | copy-start | bytes 1540
  30.0 48.8 %copy-start.2 = (f32[32]{0:T(128)S(1)}, f32[32]{0:T(128)}, u32[]{:S(2)}) copy-start(f32[32]{0:T(128)} %off_ref.1) | copy-start | bytes 388
  71.8 7.1 %collective-permute-start.1 = (bf16[32,96,128]{2,1,0:T(8,128)(2,1)S(1)}, bf16[32,96,128]{2,1,0:T(8,128)(2,1)S(1)}, u32[]{:S(2)}, u32[]{:S(2)}) collective-permute-start(bf16[32,96,128]{2,1,0:T(8,128)(2,1)S(1)} %all_to_all.17.mine_ref), channel_id=1, source_target_pairs={{0,1},{1,0},{2,3},{3,2},{4,5},{5,4},{6,7},{7,6},{8,9},{9,8},{10,11... | collective-permute-start | bytes 2359304 | tf_op jit(solution)/shard_map/ppermute | solution.py:156

commit v9 on v8

--- a/solution.py
+++ b/solution.py
@@ -52,7 +52,7 @@
 PARTS = 4
 BITS = ("z1", "z0", "y2", "y1", "y0")
 LINE = ("x1", "x0")
-WEIGHT_ORDER = ("x0", "core", "x1")
+WEIGHT_ORDER = ("core", "x0", "x1")
 CHIP_ORDER = ("x0", "x1")
 ORDER = ("y0", "y1", "z1", "z0", "y2")
 

time: 82.2 us -> 82.2 us (level)
  no operation moved by 1% of the time
where the time goes in v9:
time: 82.2 us; the launch traced here: 81.7 us
  blocking collectives  59.1 us (72%)
  starting transfers between devices  14.2 us (17%)
  Pallas kernels  4.7 us (6%)
  waiting for transfers between devices  1.89 us (2%)
  other arithmetic  0.99 us (1%)
    all_to_all x1, blocking collectives, local(): mine = lax.all_to_all(packed, ORDER, 0, 0, tiled=True)  28 us
    all_to_all x1, blocking collectives, local(): weight = lax.all_to_all(weight, WEIGHT_ORDER, 0, 0, tiled=True)  17.4 us
    all_to_all x1, blocking collectives, local(): packed = lax.all_to_all(packed, CHIP_ORDER, 0, 0, tiled=True)  13.6 us
    ppermute x1, starting transfers between devices, local(): their_rows = lax.ppermute(rows, 'core', other)  9.01 us
    ppermute x1, starting transfers between devices, local(): theirs = lax.ppermute(mine, 'core', other)  5.19 us
    pallas_call x1, Pallas kernels, read(): pl.pallas_call(read_kernel, out_shape=(jax.ShapeDtypeStruct((1, 1, span,...  2.84 us
    ppermute x1, waiting for transfers between devices, local(): theirs = lax.ppermute(mine, 'core', other)  1.89 us
    pallas_call x1, Pallas kernels, project(): pl.pallas_call(project_kernel, out_shape=jax.ShapeDtypeStruct((heads, 2 *...  1.86 us
  transfers between devices with their start and end apart: 2, of which 1 were waited for; matrix products, arithmetic and copies ran while one was open for 1% of the time, Pallas kernels for 0%

profile of v9, /device:TPU:1, one launch (start us, length us, event | category | flops | bytes accessed | tf_op | source)
XLA Modules:
  0.0 81.7 jit_solution(9962207637192353076)
XLA Ops:
  0.6 0.0 copy-start
  0.6 9.0 %collective-permute-start = (bf16[768,2048]{1,0:T(8,128)(2,1)}, bf16[768,2048]{1,0:T(8,128)(2,1)S(1)}, u32[]{:S(2)}, u32[]{:S(2)}) collective-permute-start(bf16[768,2048]{1,0:T(8,128)(2,1)} %bitcast.8), channel_id=1, source_target_pairs={{0,1},{1,0},{2,3},{3,2},{4,5},{5,4},{6,7},{7,6},{8,9},{9,8},{10,11... | collective-permute-start | bytes 9437192 | tf_op jit(solution)/shard_map/ppermute | solution.py:146
  9.7 1.0 %pad_maximum_fusion = bf16[2,256,256]{2,1,0:T(8,128)(2,1)S(1)} fusion(bf16[1,256,256]{2,1,0:T(8,128)(2,1)} %bitcast.13, bf16[1,256,256]{2,1,0:T(8,128)(2,1)} %bitcast.14), kind=kLoop, calls=%fused_computation | loop fusion | flops 131072 | bytes 524288 | tf_op jit(solution)/shard_map/stack | solution.py:147
  10.7 0.1 broadcast_in_dim.2
  10.7 17.4 %all_to_all.15.w_ref = bf16[8,256,256]{2,1,0:T(8,128)(2,1)S(1)} all-to-all(bf16[8,256,256]{2,1,0:T(8,128)(2,1)S(1)} %bitcast.10), channel_id=1, replica_groups=mesh['gr'=2,'z1'=2,'z0'=2,'y2'=2,'y1'=2,'y0'=2,'x1'=2,'x0'=2,'core'=2] {..., dimensions={0} | all-to-all | bytes 2097152 | tf_op jit(solution)/shard_map/all_to_all | solution.py:150
  28.1 0.0 collective-permute-done.other_ref
  28.1 0.0 copy-done
  28.1 1.9 %shard_map.68 = bf16[4,8,96,128]{3,2,1,0:T(8,128)(2,1)S(1)} custom-call(bf16[768,2048]{1,0:T(8,128)(2,1)S(1)} %bitcast.9, bf16[768,2048]{1,0:T(8,128)(2,1)S(1)} %collective-permute-done.other_ref, bf16[8,256,256]{2,1,0:T(8,128)(2,1)S(1)} %all_to_all.15.w_ref), custom_call_target="tpu_custom_call" | custom-call | flops 1610612736 | bytes 8388608 | tf_op jit(solution)/shard_map/pallas_call | solution.py:35
  30.0 0.0 copy-start.1
  30.0 0.0 copy-start.2
  30.0 13.6 %all_to_all.16 = bf16[4,8,96,128]{3,2,1,0:T(8,128)(2,1)S(1)} all-to-all(bf16[4,8,96,128]{3,2,1,0:T(8,128)(2,1)S(1)} %shard_map.68), channel_id=1, replica_groups=mesh['gr'=2,'z1'=2,'z0'=2,'y2'=2,'y1'=2,'y0'=2,'x1'=2,'x0'=2,'core'=2] {..., dimensions={0} | all-to-all | bytes 1572864 | tf_op jit(solution)/shard_map/all_to_all | solution.py:152
  43.6 0.1 copy.7
  43.7 28.0 %all_to_all.17.mine_ref = bf16[32,96,128]{2,1,0:T(8,128)(2,1)S(1)} all-to-all(bf16[32,96,128]{2,1,0:T(8,128)(2,1)S(1)} %bitcast.12), channel_id=1, replica_groups=mesh['gr'=2,'z1'=2,'z0'=2,'y2'=2,'y1'=2,'y0'=2,'x1'=2,'x0'=2,'core'=2] {..., dimensions={0} | all-to-all | bytes 1572864 | tf_op jit(solution)/shard_map/all_to_all | solution.py:155
  71.8 5.2 %collective-permute-start.1 = (bf16[32,96,128]{2,1,0:T(8,128)(2,1)S(1)}, bf16[32,96,128]{2,1,0:T(8,128)(2,1)S(1)}, u32[]{:S(2)}, u32[]{:S(2)}) collective-permute-start(bf16[32,96,128]{2,1,0:T(8,128)(2,1)S(1)} %all_to_all.17.mine_ref), channel_id=1, source_target_pairs={{0,1},{1,0},{2,3},{3,2},{4,5},{5,4},{6,7},{7,6},{8,9},{9,8},{10,11... | collective-permute-start | bytes 2359304 | tf_op jit(solution)/shard_map/ppermute | solution.py:156
  77.0 1.9 %collective-permute-done.1.other_ref = bf16[32,96,128]{2,1,0:T(8,128)(2,1)S(1)} collective-permute-done((bf16[32,96,128]{2,1,0:T(8,128)(2,1)S(1)}, bf16[32,96,128]{2,1,0:T(8,128)(2,1)S(1)}, u32[]{:S(2)}, u32[]{:S(2)}) %collective-permute-start.1) | collective-permute-done | bytes 786464 | tf_op jit(solution)/shard_map/ppermute | solution.py:156
  78.9 0.0 copy-done.1
  78.9 0.0 copy-done.2
  78.9 2.8 %shard_map.69 = (bf16[1,1,6144,128]{3,2,1,0:T(8,128)(2,1)}, bf16[1,4,64]{2,1,0:T(4,128)(2,1)}) custom-call(f32[32]{0:T(128)S(1)} %copy-done.2, bf16[32,96,128]{2,1,0:T(8,128)(2,1)S(1)} %all_to_all.17.mine_ref, bf16[32,96,128]{2,1,0:T(8,128)(2,1)S(1)} %collective-permute-done.1.other_ref, bf16[1,4,64]{2,1,0:T(4,128)(2,1)S(1)} %copy-done.1), custom_call_target="tpu_custom_call" | custom-call | flops 25165824 | bytes 4194304 | tf_op jit(solution)/shard_map/pallas_call | solution.py:129
Async XLA Ops:
  0.6 27.5 %copy-start = (bf16[4,192,2048]{2,1,0:T(8,128)(2,1)S(1)}, bf16[4,192,2048]{2,1,0:T(8,128)(2,1)}, u32[]{:S(2)}) copy-start(bf16[4,192,2048]{2,1,0:T(8,128)(2,1)} %param.5) | copy-start | bytes 9437188
  0.6 27.5 %collective-permute-start = (bf16[768,2048]{1,0:T(8,128)(2,1)}, bf16[768,2048]{1,0:T(8,128)(2,1)S(1)}, u32[]{:S(2)}, u32[]{:S(2)}) collective-permute-start(bf16[768,2048]{1,0:T(8,128)(2,1)} %bitcast.8), channel_id=1, source_target_pairs={{0,1},{1,0},{2,3},{3,2},{4,5},{5,4},{6,7},{7,6},{8,9},{9,8},{10,11... | collective-permute-start | bytes 9437192 | tf_op jit(solution)/shard_map/ppermute | solution.py:146
  30.0 48.9 %copy-start.1 = (bf16[1,4,64]{2,1,0:T(4,128)(2,1)S(1)}, bf16[1,4,64]{2,1,0:T(4,128)(2,1)}, u32[]{:S(2)}) copy-start(bf16[1,4,64]{2,1,0:T(4,128)(2,1)} %q_ref.1) | copy-start | bytes 1540
  30.0 48.9 %copy-start.2 = (f32[32]{0:T(128)S(1)}, f32[32]{0:T(128)}, u32[]{:S(2)}) copy-start(f32[32]{0:T(128)} %off_ref.1) | copy-start | bytes 388
  71.8 7.1 %collective-permute-start.1 = (bf16[32,96,128]{2,1,0:T(8,128)(2,1)S(1)}, bf16[32,96,128]{2,1,0:T(8,128)(2,1)S(1)}, u32[]{:S(2)}, u32[]{:S(2)}) collective-permute-start(bf16[32,96,128]{2,1,0:T(8,128)(2,1)S(1)} %all_to_all.17.mine_ref), channel_id=1, source_target_pairs={{0,1},{1,0},{2,3},{3,2},{4,5},{5,4},{6,7},{7,6},{8,9},{9,8},{10,11... | collective-permute-start | bytes 2359304 | tf_op jit(solution)/shard_map/ppermute | solution.py:156
